TPU v7x, 256 devices: a whole 4x4x8 slice. The times are simulated.
256 devices in a mesh: ep: 32 (over z, x), tp: 8 (over y, core).
Axes of the slice: x: 4, y: 4, z: 8, core: 2. Of those that a mesh axis runs over, the one named last changes fastest.
Arguments:
- tokens_first: bfloat16 [16384, 2048], P('ep'), may hold values from -6 to 6
- attn_gain: float32 [2048], replicated, may hold values from 0.1 to 1.9
- w_query: bfloat16 [2048, 1024], P(None, 'tp'), may hold values from -6 to 6
- key_matrix: bfloat16 [2048, 512], P(None, 'tp'), may hold values from -6 to 6
- value_matrix: bfloat16 [2048, 512], P(None, 'tp'), may hold values from -0.125 to 0.125
- head_sink_logit: float32 [16], P('tp'), may hold values from 1 to 5
- w_output: bfloat16 [1024, 2048], P('tp'), may hold values from -0.75 to 0.75
- tokens_second: bfloat16 [4096, 2048], P('ep'), may hold values from -6 to 6
- ffn_gain: float32 [2048], replicated, may hold values from 0.1 to 1.9
- routes: int32 [4096, 4], P('ep'), may hold values from 0 to 63, all different within a row; in each aligned block of 128 rows (0 to 127, 128 to 255, ...) at most 16 rows name the same one
- route_weight: float32 [4096, 4], P('ep'), may hold values from 0.2 to 1.5
- w_gate_exp: bfloat16 [64, 2048, 2048], P('ep', None, 'tp'), may hold values from -0.125 to 0.125
- w_up_exp: bfloat16 [64, 2048, 2048], P('ep', None, 'tp'), may hold values from -0.125 to 0.125
- w_down_exp: bfloat16 [64, 2048, 2048], P('ep', 'tp'), may hold values from -0.125 to 0.125
- w_gate_shared: bfloat16 [2048, 1024], P(None, 'tp'), may hold values from -0.125 to 0.125
- w_up_shared: bfloat16 [2048, 1024], P(None, 'tp'), may hold values from -0.125 to 0.125
- w_down_shared: bfloat16 [1024, 2048], P('tp'), may hold values from -0.1875 to 0.1875
Outputs:
- mixer_out: bfloat16 [16384, 2048], P(('ep', 'tp'))
- moe_out: bfloat16 [4096, 2048], P('ep', 'tp')
Inputs may be any that keep to these rules, and one draw needn't show every extreme that they name: `routes`: each row names 4 different experts; among the rows of one index of ep no expert is named more than 16 times, a bound that some block reaches.
All inputs are finite; a program needn't handle non-finite values.
Results may differ from a plain program's by a relative error of at most 0.017.
Values may be sent and summed in bfloat16 or wider, within the bound.
A program may use at most 64 MiB of HBM per device.

v0:
```python
import jax
import jax.numpy as jnp
from jax import lax
from jax.sharding import PartitionSpec as P

MODEL_WIDTH = 2048
HEAD_SIZE = 64
BAND_LENGTH = 128


rope_base = 10000.0
norm_eps = 1e-06


def from_behind(value, axis, by):
    devices = lax.axis_size(axis)
    pairs = [(i, i + by) for i in range(devices) if 0 <= i + by < devices]
    return lax.ppermute(value, axis, pairs)


def cut_along(value, dim, devices):
    dims = value.shape
    blocks = value.reshape(*dims[:dim], devices, dims[dim] // devices, *dims[dim + 1 :])
    return jnp.moveaxis(blocks, dim, 0)


def sent_and_summed(value, axis, dim):
    devices = lax.axis_size(axis)
    blocks = lax.all_to_all(cut_along(value, dim, devices), axis, 0, 0, tiled=True)
    return jnp.sum(blocks.astype(jnp.float32), axis=0)


def rms_scale(inputs, gain):
    wide = inputs.astype(jnp.float32)
    scaled = wide * lax.rsqrt(jnp.mean(wide * wide, axis=-1, keepdims=True) + norm_eps)
    return (scaled * gain).astype(jnp.bfloat16)


def apply_rotary(heads, token_positions):
    freqs = rope_base ** (-jnp.arange(0, HEAD_SIZE, 2, dtype=jnp.float32) / HEAD_SIZE)
    angles = token_positions[:, None] * freqs[None, :]
    cosine = jnp.cos(angles)[:, None, :]
    sine = jnp.sin(angles)[:, None, :]
    first_half, second_half = jnp.split(heads, 2, axis=-1)
    return jnp.concatenate(
        [first_half * cosine - second_half * sine, second_half * cosine + first_half * sine],
        axis=-1,
    )


def local(
    tokens_first,
    attn_gain,
    w_query,
    key_matrix,
    value_matrix,
    head_sink_logit,
    w_output,
    tokens_second,
    ffn_gain,
    routes,
    route_weight,
    w_gate_exp,
    w_up_exp,
    w_down_exp,
    w_gate_shared,
    w_up_shared,
    w_down_shared,
):
    rows_first = tokens_first.shape[0]
    norm_input = rms_scale(tokens_first, attn_gain)
    offset = lax.axis_index("ep") * rows_first
    token_positions = (offset + jnp.arange(rows_first, dtype=jnp.int32)).astype(jnp.float32)
    head_count = w_query.shape[1] // HEAD_SIZE
    key_heads = key_matrix.shape[1] // HEAD_SIZE
    head_group = head_count // key_heads
    query_rows = apply_rotary(
        jnp.dot(norm_input, w_query, preferred_element_type=jnp.float32).reshape(
            rows_first, head_count, HEAD_SIZE
        ),
        token_positions,
    ).astype(jnp.bfloat16)
    keys_local = apply_rotary(
        jnp.dot(norm_input, key_matrix, preferred_element_type=jnp.float32).reshape(
            rows_first, key_heads, HEAD_SIZE
        ),
        token_positions,
    ).astype(jnp.bfloat16)
    values_local = (
        jnp.dot(norm_input, value_matrix, preferred_element_type=jnp.float32)
        .astype(jnp.bfloat16)
        .reshape(rows_first, key_heads, HEAD_SIZE)
    )
    keys_before, values_before = from_behind(
        (keys_local[rows_first - BAND_LENGTH :], values_local[rows_first - BAND_LENGTH :]), "ep", 1
    )
    keys_all = jnp.concatenate([keys_before, keys_local], axis=0)
    values_all = jnp.concatenate([values_before, values_local], axis=0)
    layer_block = min(512, rows_first)
    sink_scores = head_sink_logit.reshape(key_heads, head_group)[:, :, None, None]

    def attend(index):
        leading_row = index * layer_block
        block_queries = query_rows.reshape(layer_block, key_heads, head_group, HEAD_SIZE)
        scores = jnp.einsum(
            "qhgd,khd->hgqk", block_queries, keys_all, preferred_element_type=jnp.float32
        ) * HEAD_SIZE ** (-0.5)
        query_pos = offset + leading_row + jnp.arange(layer_block, dtype=jnp.int32)
        key_pos = (
            offset
            + leading_row
            - BAND_LENGTH
            + jnp.arange(layer_block + BAND_LENGTH, dtype=jnp.int32)
        )
        offsets = query_pos[:, None] - key_pos[None, :]
        visible = (offsets >= 0) & (offsets < BAND_LENGTH) & (key_pos[None, :] >= 0)
        scores = jnp.where(visible[None, None], scores, -jnp.inf)
        peak = jnp.maximum(jnp.max(scores, axis=-1, keepdims=True), sink_scores)
        expo = jnp.exp(scores - peak)
        total = jnp.sum(expo, axis=-1, keepdims=True) + jnp.exp(sink_scores - peak)
        weights = (expo / total).astype(jnp.bfloat16)
        mixed = jnp.einsum(
            "hgqk,khd->qhgd", weights, values_all, preferred_element_type=jnp.float32
        )
        return mixed.astype(jnp.bfloat16).reshape(layer_block, head_count * HEAD_SIZE)

    attended = lax.map(attend, jnp.arange(rows_first // layer_block, dtype=jnp.int32)).reshape(
        rows_first, head_count * HEAD_SIZE
    )
    mixer_out = sent_and_summed(
        jnp.dot(attended, w_output, preferred_element_type=jnp.float32).astype(jnp.bfloat16),
        "tp",
        0,
    ).astype(jnp.bfloat16)
    rows_second = tokens_second.shape[0]
    topk = routes.shape[1]
    exp_dev = w_gate_exp.shape[0]
    n_expdev = lax.axis_size("ep")
    experts = exp_dev * n_expdev
    capacity = max(2, 2 * rows_second * topk // experts)
    slot_count = experts * capacity
    normed_second = rms_scale(tokens_second, ffn_gain)
    flat = routes.reshape(-1)
    onehot = (flat[:, None] == jnp.arange(experts, dtype=jnp.int32)[None, :]).astype(jnp.int32)
    ranks = jnp.sum((jnp.cumsum(onehot, axis=0) - onehot) * onehot, axis=1)
    slots = flat * capacity + ranks
    match = (jnp.arange(slot_count, dtype=jnp.int32)[:, None] == slots[None, :]).reshape(
        slot_count, rows_second, topk
    )
    dispatch = jnp.sum(match.astype(jnp.float32), axis=2).astype(jnp.bfloat16)
    combine = jnp.sum(match.astype(jnp.float32) * route_weight[None, :, :], axis=2)
    width = normed_second.shape[1] // lax.axis_size("tp")
    feature_slice = lax.dynamic_slice_in_dim(normed_second, lax.axis_index("tp") * width, width, 1)
    outgoing = jnp.dot(dispatch, feature_slice, preferred_element_type=jnp.float32).astype(
        jnp.bfloat16
    )
    arrived = lax.all_to_all(outgoing, "ep", split_axis=0, concat_axis=0, tiled=True)
    piece = lax.all_gather(arrived, "tp", axis=1, tiled=True)
    cols = piece.shape[1]
    part = piece.reshape(n_expdev, exp_dev, capacity, cols)
    gate_pre = jnp.einsum("sjcd,jdf->sjcf", part, w_gate_exp, preferred_element_type=jnp.float32)
    up_pre = jnp.einsum("sjcd,jdf->sjcf", part, w_up_exp, preferred_element_type=jnp.float32)
    hidden = (jax.nn.silu(gate_pre) * up_pre).astype(jnp.bfloat16)
    shared_hidden = (
        jax.nn.silu(jnp.dot(normed_second, w_gate_shared, preferred_element_type=jnp.float32))
        * jnp.dot(normed_second, w_up_shared, preferred_element_type=jnp.float32)
    ).astype(jnp.bfloat16)
    routed_term = jnp.einsum(
        "sjcf,jfd->dsjc", hidden, w_down_exp, preferred_element_type=jnp.float32
    ).reshape(lax.axis_size("tp") * (MODEL_WIDTH // lax.axis_size("tp")), slot_count)
    shared_term = lax.dot_general(
        w_down_shared, shared_hidden, (((0,), (1,)), ((), ())), preferred_element_type=jnp.float32
    )
    summed = lax.psum_scatter(
        jnp.concatenate([routed_term, shared_term], axis=1).astype(jnp.bfloat16),
        "tp",
        scatter_dimension=0,
        tiled=True,
    ).astype(jnp.float32)
    routed_part = summed[:, :slot_count].astype(jnp.bfloat16)
    returned = lax.all_to_all(routed_part, "ep", split_axis=1, concat_axis=1, tiled=True)
    weighted = lax.dot_general(combine, returned.astype(jnp.float32), (((0,), (1,)), ((), ())))
    moe_out = (weighted + summed[:, slot_count:].T).astype(jnp.bfloat16)
    return (mixer_out, moe_out)


def solution(mesh):
    in_specs = (
        P("ep", None),
        P(),
        P(None, "tp"),
        P(None, "tp"),
        P(None, "tp"),
        P("tp"),
        P("tp", None),
        P("ep", None),
        P(),
        P("ep", None),
        P("ep", None),
        P("ep", None, "tp"),
        P("ep", None, "tp"),
        P("ep", "tp", None),
        P(None, "tp"),
        P(None, "tp"),
        P("tp", None),
    )
    out_specs = (P(("ep", "tp"), None), P("ep", "tp"))
    return jax.shard_map(local, mesh=mesh, in_specs=in_specs, out_specs=out_specs, check_vma=False)
```

profile of v0, /device:TPU:2, one launch (start us, length us, event | category | flops | bytes accessed | tf_op | source)
XLA Modules:
  0.0 193.0 jit_solution(15909732871255852023)
XLA Ops:
  8.4 1.2 reduce-window.6
  10.9 1.2 fusion.42
  12.1 1.1 convert_reduce_fusion
  13.2 1.2 fusion.44
  14.8 28.3 %all_to_all.29 = bf16[32,32,256]{2,1,0:T(8,128)(2,1)} all-to-all(bf16[32,32,256]{2,1,0:T(8,128)(2,1)S(1)} %bitcast.128), channel_id=1, replica_groups=mesh['ep'=32,'tp'=8] {'ep'}, dimensions={0} | all-to-all | bytes 1048576 | tf_op jit(solution)/shard_map/all_to_all | solution.py:157
  43.2 1.3 fusion.92
  44.5 1.7 fusion.7
  46.3 32.0 %all-gather.2.cloned.1.call-done = bf16[1024,2048]{1,0:T(8,128)(2,1)} async-done(((bf16[1024,256]{1,0:T(8,128)(2,1)}), bf16[1024,2048]{1,0:T(8,128)(2,1)}) %all-gather.2.cloned.1.call-update) | async-done | bytes 4194320 | tf_op jit(solution)/shard_map/all_gather | solution.py:158
  78.3 5.2 %fusion.13 = f32[32,2,16,256]{3,2,0,1:T(8,128)} fusion(bf16[2,2048,256]{2,1,0:T(8,128)(2,1)} %param.28, bf16[32,2,16,2048]{3,2,1,0:T(8,128)(2,1)} %bitcast.132), kind=kOutput, calls=%fused_computation.27 | convolution fusion | flops 1073741824 | bytes 7340032 | tf_op jit(solution)/shard_map/sjcd,jdf->sjcf/dot_general | solution.py:161
  83.5 7.5 %convert_bitcast_fusion = bf16[2048,32,2,16]{0,3,1,2:T(8,128)(2,1)} fusion(bf16[2,256,2048]{2,1,0:T(8,128)(2,1)S(1)} %copy-done, bf16[2,2048,256]{2,1,0:T(8,128)(2,1)} %param.29, bf16[32,2,16,2048]{3,2,1,0:T(8,128)(2,1)} %bitcast.133, f32[32,2,16,256]{3,2,0,1:T(8,128)} %fusion.13), kind=kOutput, calls=%fused_computation.6 | convolution fusion | flops 2151153664 | bytes 13631488 | tf_op jit(solution)/shard_map/sjcf,jfd->dsjc/dot_general | solution.py:168
  91.0 2.5 %copy.48 = bf16[2048,32,2,16]{0,3,2,1:T(8,128)(2,1)S(1)} copy(bf16[2048,32,2,16]{0,3,1,2:T(8,128)(2,1)} %convert_bitcast_fusion) | data formatting | bytes 8388608 | tf_op jit(solution)/shard_map/sjcf,jfd->dsjc/transpose | solution.py:168
  93.5 2.5 %pad_maximum_fusion = bf16[2048,1152]{0,1:T(8,128)(2,1)} fusion(bf16[2048,128]{0,1:T(8,128)(2,1)S(1)} %fusion.7, bf16[2048,1024]{0,1:T(8,128)(2,1)S(1)} %bitcast.124), kind=kLoop, calls=%fused_computation.2 | loop fusion | flops 9437184 | bytes 9437184 | tf_op jit(solution)/shard_map/concatenate | solution.py:175
  96.0 2.2 %fusion = f32[512]{0:T(512)S(1)} fusion(bf16[512,2048]{1,0:T(8,128)(2,1)} %param.17), kind=kLoop, calls=%fused_computation.3 | loop fusion | flops 3145216 | bytes 2099200 | tf_op jit(solution)/shard_map/reduce_sum | solution.py:35
  100.3 3.4 %collective-permute-start.1 = (bf16[128,1,64]{0,2,1:T(8,128)(2,1)S(1)}, bf16[128,1,64]{0,2,1:T(8,128)(2,1)S(1)}, u32[]{:S(2)}, u32[]{:S(2)}) collective-permute-start(bf16[128,1,64]{0,2,1:T(8,128)(2,1)S(1)} %pad_maximum_fusion.1), channel_id=1, source_target_pairs={{0,8},{8,16},{16,24},{24,32},{32,40},{40,48},{48,56},{56,64},{64,7... | collective-permute-start | bytes 49160 | tf_op jit(solution)/shard_map/ppermute | solution.py:18
  104.5 3.3 %collective-permute-start = (bf16[128,1,64]{0,2,1:T(8,128)(2,1)S(1)}, bf16[128,1,64]{0,2,1:T(8,128)(2,1)S(1)}, u32[]{:S(2)}, u32[]{:S(2)}) collective-permute-start(bf16[128,1,64]{0,2,1:T(8,128)(2,1)S(1)} %slice_bitcast_fusion), channel_id=1, source_target_pairs={{0,8},{8,16},{16,24},{24,32},{32,40},{40,48},{48,56},{56,64},{64,7... | collective-permute-start | bytes 49160 | tf_op jit(solution)/shard_map/ppermute | solution.py:18
  108.1 2.6 %fusion.91 = f32[512,128]{0,1:T(8,128)S(1)} fusion(bf16[512,2048]{1,0:T(8,128)(2,1)} %copy-done.1, bf16[2048,128]{1,0:T(8,128)(2,1)S(1)} %copy-done.3), kind=kOutput, calls=%fused_computation.114 | convolution fusion | flops 268435456 | bytes 2883584 | tf_op jit(solution)/shard_map/dot_general | solution.py:78
  113.7 2.1 %convolution_convert_fusion = bf16[512,2048]{1,0:T(8,128)(2,1)} fusion(bf16[512,128]{0,1:T(8,128)(2,1)S(1)} %bitcast.130, bf16[128,2048]{1,0:T(8,128)(2,1)S(1)} %copy-done.4), kind=kOutput, calls=%fused_computation.11 | convolution fusion | flops 269484032 | bytes 2752512 | tf_op jit(solution)/shard_map/dot_general | solution.py:131
  115.8 4.4 %all-to-all-start = ((bf16[8,64,2048]{2,1,0:T(8,128)(2,1)}), bf16[8,64,2048]{2,1,0:T(8,128)(2,1)}, u32[]{:S(2)}, u32[]{:S(2)}) async-start(bf16[8,64,2048]{2,1,0:T(8,128)(2,1)} %bitcast.125), calls=%async_computation | async-start | bytes 4194304 | tf_op jit(solution)/shard_map/all_to_all | solution.py:29
  120.2 38.9 %reduce-scatter.2.cloned.1.call-done = bf16[256,1152]{0,1:T(8,128)(2,1)} async-done(((bf16[2048,1152]{0,1:T(8,128)(2,1)}), bf16[256,1152]{0,1:T(8,128)(2,1)}) %reduce-scatter.2.cloned.1.call-update) | async-done | bytes 589840 | tf_op jit(solution)/shard_map/reduce_scatter | solution.py:174
  159.1 1.9 slice.32
  161.0 9.6 %all-to-all-start.2 = ((bf16[256,32,32]{0,2,1:T(8,128)(2,1)}), bf16[256,32,32]{0,2,1:T(8,128)(2,1)S(1)}, u32[]{:S(2)}, u32[]{:S(2)}) async-start(bf16[256,32,32]{0,2,1:T(8,128)(2,1)} %bitcast.30), calls=%async_computation.3 | async-start | bytes 1048576 | tf_op jit(solution)/shard_map/all_to_all | solution.py:181
  170.6 2.7 %reduce_sum.71 = bf16[64,2048]{1,0:T(8,128)(2,1)} reduce(bf16[8,64,2048]{2,1,0:T(8,128)(2,1)} %all-to-all-done, bf16[]{:T(256)} %constant.71.clone.1), dimensions={0}, to_apply=%region_3.4 | reduce | flops 917504 | bytes 2359298 | tf_op jit(solution)/shard_map/reduce_sum | solution.py:30
  173.4 11.0 %all-to-all-done.2 = bf16[256,32,32]{0,2,1:T(8,128)(2,1)S(1)} async-done(((bf16[256,32,32]{0,2,1:T(8,128)(2,1)}), bf16[256,32,32]{0,2,1:T(8,128)(2,1)S(1)}, u32[]{:S(2)}, u32[]{:S(2)}) %all-to-all-start.2) | async-done | bytes 524320 | tf_op jit(solution)/shard_map/all_to_all | solution.py:181
  184.4 1.7 fusion.40
  (58 shorter events, 8.9 us)
Async XLA Ops:
  7.2 76.3 %copy-start = (bf16[2,256,2048]{2,1,0:T(8,128)(2,1)S(1)}, bf16[2,256,2048]{2,1,0:T(8,128)(2,1)}, u32[]{:S(2)}) copy-start(bf16[2,256,2048]{2,1,0:T(8,128)(2,1)} %param.30) | copy-start | bytes 6291460
  7.2 71.1 %all-gather.2.cloned.1.call-start = ((), (), s32[]{:S(2)}) async-start(), calls=%async_computation.4 | async-start | bytes 4718592 | tf_op jit(solution)/shard_map/all_gather | solution.py:158
  43.1 116.0 %reduce-scatter.2.cloned.1.call-start = ((), (), s32[]{:S(2)}) async-start(), calls=%async_computation.5 | async-start | bytes 5308416 | tf_op jit(solution)/shard_map/reduce_scatter | solution.py:174
  96.0 2.3 %copy-start.7 = (f32[2048]{0:T(1024)S(1)}, f32[2048]{0:T(1024)}, u32[]{:S(2)}) copy-start(f32[2048]{0:T(1024)} %param.18) | copy-start | bytes 24580
  96.0 2.3 %copy-start.2 = (bf16[512,2048]{1,0:T(8,128)(2,1)S(1)}, bf16[512,2048]{1,0:T(8,128)(2,1)}, u32[]{:S(2)}) copy-start(bf16[512,2048]{1,0:T(8,128)(2,1)} %param.17) | copy-start | bytes 6291460
  98.3 1.0 copy-start.5
  98.3 5.4 %copy-start.6 = (bf16[2048,64]{0,1:T(8,128)(2,1)S(1)}, bf16[2048,64]{0,1:T(8,128)(2,1)}, u32[]{:S(2)}) copy-start(bf16[2048,64]{0,1:T(8,128)(2,1)} %param.21) | copy-start | bytes 786436
  99.2 4.5 %copy-start.1 = (bf16[512,2048]{1,0:T(8,128)(2,1)}, bf16[512,2048]{1,0:T(8,128)(2,1)S(1)}, u32[]{:S(2)}) copy-start(bf16[512,2048]{1,0:T(8,128)(2,1)S(1)} %fusion.2) | copy-start | bytes 6291460
  99.2 8.9 %copy-start.3 = (bf16[2048,128]{1,0:T(8,128)(2,1)S(1)}, bf16[2048,128]{1,0:T(8,128)(2,1)}, u32[]{:S(2)}) copy-start(bf16[2048,128]{1,0:T(8,128)(2,1)} %param.19) | copy-start | bytes 1572868
  100.3 10.9 %collective-permute-start.1 = (bf16[128,1,64]{0,2,1:T(8,128)(2,1)S(1)}, bf16[128,1,64]{0,2,1:T(8,128)(2,1)S(1)}, u32[]{:S(2)}, u32[]{:S(2)}) collective-permute-start(bf16[128,1,64]{0,2,1:T(8,128)(2,1)S(1)} %pad_maximum_fusion.1), channel_id=1, source_target_pairs={{0,8},{8,16},{16,24},{24,32},{32,40},{40,48},{48,56},{56,64},{64,7... | collective-permute-start | bytes 49160 | tf_op jit(solution)/shard_map/ppermute | solution.py:18
  104.5 8.2 %collective-permute-start = (bf16[128,1,64]{0,2,1:T(8,128)(2,1)S(1)}, bf16[128,1,64]{0,2,1:T(8,128)(2,1)S(1)}, u32[]{:S(2)}, u32[]{:S(2)}) collective-permute-start(bf16[128,1,64]{0,2,1:T(8,128)(2,1)S(1)} %slice_bitcast_fusion), channel_id=1, source_target_pairs={{0,8},{8,16},{16,24},{24,32},{32,40},{40,48},{48,56},{56,64},{64,7... | collective-permute-start | bytes 49160 | tf_op jit(solution)/shard_map/ppermute | solution.py:18
  110.7 1.2 copy-start.8
  112.6 1.1 copy-start.4
  115.8 45.2 %all-to-all-start = ((bf16[8,64,2048]{2,1,0:T(8,128)(2,1)}), bf16[8,64,2048]{2,1,0:T(8,128)(2,1)}, u32[]{:S(2)}, u32[]{:S(2)}) async-start(bf16[8,64,2048]{2,1,0:T(8,128)(2,1)} %bitcast.125), calls=%async_computation | async-start | bytes 4194304 | tf_op jit(solution)/shard_map/all_to_all | solution.py:29
  161.0 23.4 %all-to-all-start.2 = ((bf16[256,32,32]{0,2,1:T(8,128)(2,1)}), bf16[256,32,32]{0,2,1:T(8,128)(2,1)S(1)}, u32[]{:S(2)}, u32[]{:S(2)}) async-start(bf16[256,32,32]{0,2,1:T(8,128)(2,1)} %bitcast.30), calls=%async_computation.3 | async-start | bytes 1048576 | tf_op jit(solution)/shard_map/all_to_all | solution.py:181
Sparse Core Ops, SparseCore 0:
  43.3 34.9 all-gather.1
  96.1 62.9 reduce-scatter.1
where the time goes:
time: 195 us; the launch traced here: 193 us
  waiting for transfers between devices  82 us (42%)
  blocking collectives  28.3 us (15%)
  matrix products  25.6 us (13%)
  starting transfers between devices  20.7 us (11%)
  other arithmetic  15.6 us (8%)
  between operations  14.4 us (7%)
  local copies, waits for them, and re-layouts  6.4 us (3%)
    reduce_scatter x1, waiting for transfers between devices, local(): lax.psum_scatter(jnp.concatenate([routed_term, shared_term], axis=1).asty...  38.9 us
    all_gather x1, waiting for transfers between devices, local(): piece = lax.all_gather(arrived, 'tp', axis=1, tiled=True)  32 us
    all_to_all x1, blocking collectives, local(): lax.all_to_all(outgoing, 'ep', split_axis=0, concat_axis=0, tiled=True)  28.3 us
    all_to_all x1, waiting for transfers between devices, local(): lax.all_to_all(routed_part, 'ep', split_axis=1, concat_axis=1, tiled=True)  11 us
    all_to_all x1, starting transfers between devices, local(): lax.all_to_all(routed_part, 'ep', split_axis=1, concat_axis=1, tiled=True)  9.63 us
    dot_general x1, matrix products, local(): jnp.einsum('sjcf,jfd->dsjc', hidden, w_down_exp, preferred_element_type=j...  7.5 us
    ppermute x2, starting transfers between devices, from_behind(): return lax.ppermute(value, axis, pairs)  6.64 us
    dot_general x1, matrix products, local(): jnp.einsum('sjcd,jdf->sjcf', part, w_gate_exp, preferred_element_type=jnp...  5.18 us
  transfers between devices with their start and end apart: 6, of which 3 were waited for; matrix products, arithmetic and copies ran while one was open for 10% of the time, Pallas kernels for 0%

commit v1 on v0

v1 whole, which is shorter than its diff:
```python
import functools

import jax
import jax.numpy as jnp
import numpy as np
from jax import lax
from jax.experimental import pallas as pl
from jax.experimental.pallas import tpu as pltpu
from jax.sharding import PartitionSpec as P

HEAD = 64
BAND = 128
CAP = 16
NX = 4
NY = 4
ROPE_BASE = 10000.0
EPS = 1e-06
MESH = pl.DeviceIdType.MESH
F32 = jnp.float32
BF16 = jnp.bfloat16


def z_order(nz):
    out = [0]
    for d in range(1, nz // 2 + 1):
        out.append(d)
        if d != nz - d:
            out.append(-d)
    return out


def rope_tables(rows, n_ep):
    freqs = ROPE_BASE ** (-np.arange(0, HEAD, 2, dtype=np.float64) / HEAD)
    lanes = np.tile(freqs, 4)[None, :]
    within = np.arange(rows, dtype=np.float64)[:, None] * lanes
    starts = np.arange(n_ep, dtype=np.float64)[:, None] * rows * lanes
    return tuple(
        np.asarray(t, np.float32) for t in (np.cos(within), np.sin(within), np.cos(starts), np.sin(starts))
    )


def kernel(cfg, *refs):
    nz, nx, n_tp, d_model, t1, t2, topk, eff, sff = cfg
    n_in = 21
    (
        tok1_h, gain1_h, wq_h, wk_h, wv_h, sink_h, wo_h, tok2_h, gain2_h, routes_h, rw_h,
        wg_h, wu_h, wd_h, sg_h, su_h, sd_h, cosb_h, sinb_h, cosa_h, sina_h,
    ) = refs[:n_in]
    mix_h, moe_h = refs[n_in : n_in + 2]
    (
        tok1, gain1, wq, wk, wv, sink, wo, tok2, gain2, routes, rw,
        wg, wu, wd, sg, su, sd, cosb, sinb, cosa, sina,
    ) = refs[n_in + 2 : 2 * n_in + 2]
    (
        n2, onehot, comb, outgoing, xs, nrm, qs, kv, wkv, pm, pmr, r2m, r1m, p_ref, pr, r2, r1, y_ref, ret, shr,
        acc, mix_o, moe_o,
        load_sem, halo_s, halo_r, dsp_s, dsp_r, ag_s, ag_r, rs_s, rs_r, mx_s, mx_r, rt_s, rt_r, st_sem,
    ) = refs[2 * n_in + 2 :]
    f = d_model // n_tp
    n_ep = nz * nx
    order = z_order(nz)
    chunks = nz // 2
    groups = p_ref.shape[3]
    slot_groups = 2 * nx
    half = (groups + 1) // 2
    s_rows = t2 // chunks

    ep = lax.axis_index("ep")
    tp = lax.axis_index("tp")
    z, x = ep // nx, ep % nx
    y, c = tp // 2, tp % 2
    partner = y * 2 + (1 - c)
    y_up, y_dn, y_far = (y + 1) % NY, (y + NY - 1) % NY, (y + 2) % NY
    up, dn, far = y_up * 2 + c, y_dn * 2 + c, y_far * 2 + c

    hbm = (tok1_h, gain1_h, wq_h, wk_h, wv_h, sink_h, wo_h, tok2_h, gain2_h, routes_h, rw_h,
           wg_h, wu_h, wd_h, sg_h, su_h, sd_h, cosb_h, sinb_h, cosa_h, sina_h)
    vmem = (tok1, gain1, wq, wk, wv, sink, wo, tok2, gain2, routes, rw,
            wg, wu, wd, sg, su, sd, cosb, sinb, cosa, sina)
    loads = [pltpu.make_async_copy(h, v, load_sem.at[i]) for i, (h, v) in enumerate(zip(hbm, vmem))]
    for i in (7, 8, 9, 10, 0, 1, 2, 3, 4, 5, 17, 18, 19, 20, 6, 14, 15, 16, 11, 12, 13):
        loads[i].start()

    barrier = pltpu.get_barrier_semaphore()
    for dz in range(nz):
        for dx in range(nx):
            if dz or dx:
                peer = ((z + dz) % nz) * nx + (x + dx) % nx
                pl.semaphore_signal(barrier, inc=1, device_id=(peer, tp), device_id_type=MESH)
    for other in (up, dn, partner):
        pl.semaphore_signal(barrier, inc=1, device_id=(ep, other), device_id_type=MESH)

    sends = []

    def send(src, dst, ssem, rsem, to_ep, to_tp):
        copy = pltpu.make_async_remote_copy(
            src_ref=src, dst_ref=dst, send_sem=ssem, recv_sem=rsem, device_id=(to_ep, to_tp), device_id_type=MESH
        )
        copy.start()
        sends.append((src, ssem))

    def arrived(dst, rsem):
        pltpu.make_async_copy(dst, dst, rsem).wait()

    for i in (7, 8, 9, 10):
        loads[i].wait()

    wide = tok2[...].astype(F32)
    scale = lax.rsqrt(jnp.mean(wide * wide, axis=-1, keepdims=True) + EPS)
    normed = (wide * scale * gain2[...]).astype(BF16)
    for j in range(n_tp):
        n2[j] = normed[:, j * f : (j + 1) * f]

    lane = lax.broadcasted_iota(jnp.int32, (t2, 128), 1)
    named = jnp.zeros((t2, 128), F32)
    weight = jnp.zeros((t2, 128), F32)
    for k in range(topk):
        hit = lane == routes[:, k : k + 1]
        named = jnp.where(hit, 1.0, named)
        weight = jnp.where(hit, rw[:, k : k + 1], weight)
    named_t = named.T
    row_i = lax.broadcasted_iota(jnp.int32, (t2, t2), 0)
    col_i = lax.broadcasted_iota(jnp.int32, (t2, t2), 1)
    before = jnp.where(row_i < col_i, 1.0, 0.0).astype(BF16)
    rank_t = jnp.dot(named_t.astype(BF16), before, preferred_element_type=F32)
    rank_t = jnp.where(named_t > 0.5, rank_t, -1.0)[: 2 * n_ep]
    cap_i = lax.broadcasted_iota(jnp.int32, (2 * n_ep, CAP, t2), 1).astype(F32)
    dispatch = jnp.where(rank_t[:, None, :] == cap_i, 1.0, 0.0).astype(BF16).reshape(2 * n_ep * CAP, t2)
    sent = jnp.dot(dispatch, n2[tp], preferred_element_type=F32).astype(BF16)
    outgoing[...] = sent.reshape(n_ep, 2, CAP, f)

    pl.semaphore_wait(barrier, n_ep - 1 + 3)

    xs[0, tp, x] = outgoing[ep]
    for p, dz in enumerate(order):
        to_z = (z + nz - dz) % nz
        for i in range(nx):
            if p == 0 and i == 0:
                continue
            to = to_z * nx + (x + i) % nx
            pltpu.make_async_remote_copy(
                src_ref=outgoing.at[to], dst_ref=xs.at[p // 2, tp, (p % 2) * nx + x], send_sem=dsp_s,
                recv_sem=dsp_r.at[p // 2], device_id=(to, tp), device_id_type=MESH,
            ).start()

    after = jnp.where(row_i > col_i, 1.0, 0.0).astype(BF16)
    rank = jnp.dot(after, named.astype(BF16), preferred_element_type=F32)
    rank = jnp.where(named > 0.5, rank, -1.0).astype(BF16)
    w_hi = weight.astype(BF16)
    w_lo = (weight - w_hi.astype(F32)).astype(BF16)
    per_z = 2 * nx * CAP
    for zz in range(nz):
        e_row = lax.broadcasted_iota(jnp.int32, (128, per_z), 0)
        e_col = lax.broadcasted_iota(jnp.int32, (128, per_z), 1)
        spread = jnp.where(e_row == zz * 2 * nx + e_col // CAP, 1.0, 0.0).astype(BF16)
        slot = (lax.broadcasted_iota(jnp.int32, (t2, per_z), 1) % CAP).astype(F32)
        mine = jnp.dot(rank, spread, preferred_element_type=F32) == slot
        comb[zz, 0] = jnp.where(mine, jnp.dot(w_hi, spread, preferred_element_type=F32), 0.0).astype(BF16)
        comb[zz, 1] = jnp.where(mine, jnp.dot(w_lo, spread, preferred_element_type=F32), 0.0).astype(BF16)

    slot_half = slot_groups // 2

    def gather_start(k):
        first = 1 if k == 0 else 0
        arrived(xs.at[k, 0, pl.ds(0, slot_groups - first)], dsp_r.at[k])
        own = xs.at[k, tp]
        send(own, own, ag_s.at[k, 0], ag_r.at[k, 0], ep, up)
        send(own, own, ag_s.at[k, 1], ag_r.at[k, 1], ep, dn)
        send(own, own, ag_s.at[k, 2], ag_r.at[k, 2], ep, partner)

    def gather_forward(k):
        low, high = pl.ds(0, slot_half), pl.ds(slot_half, slot_half)
        arrived(xs.at[k, dn], ag_r.at[k, 0])
        send(xs.at[k, dn, low], xs.at[k, dn, low], ag_s.at[k, 3], ag_r.at[k, 3], ep, up)
        send(xs.at[k, dn], xs.at[k, dn], ag_s.at[k, 5], ag_r.at[k, 5], ep, partner)
        arrived(xs.at[k, up], ag_r.at[k, 1])
        send(xs.at[k, up, high], xs.at[k, up, high], ag_s.at[k, 4], ag_r.at[k, 4], ep, dn)
        send(xs.at[k, up], xs.at[k, up], ag_s.at[k, 6], ag_r.at[k, 6], ep, partner)

    def gather_far(k):
        low, high = pl.ds(0, slot_half), pl.ds(slot_half, slot_half)
        arrived(xs.at[k, far, low], ag_r.at[k, 3])
        send(xs.at[k, far, low], xs.at[k, far, low], ag_s.at[k, 7], ag_r.at[k, 7], ep, partner)
        arrived(xs.at[k, far, high], ag_r.at[k, 4])
        send(xs.at[k, far, high], xs.at[k, far, high], ag_s.at[k, 8], ag_r.at[k, 8], ep, partner)

    def gather_end(k):
        low, high = pl.ds(0, slot_half), pl.ds(slot_half, slot_half)
        other = 1 - c
        arrived(xs.at[k, partner], ag_r.at[k, 2])
        arrived(xs.at[k, y_dn * 2 + other], ag_r.at[k, 5])
        arrived(xs.at[k, y_up * 2 + other], ag_r.at[k, 6])
        arrived(xs.at[k, y_far * 2 + other, low], ag_r.at[k, 7])
        arrived(xs.at[k, y_far * 2 + other, high], ag_r.at[k, 8])

    def pair_send(part, got, ss, rs, targets):
        for o in targets:
            t = (y + o) % NY
            send(part.at[t, 1 - c], got.at[t], ss.at[o], rs.at[o], ep, partner)

    def pair_sum(part, got, rs, o):
        t = (y + o) % NY
        arrived(got.at[t], rs.at[o])
        part[t, c] = (part[t, c].astype(F32) + got[t].astype(F32)).astype(BF16)

    def ring_first(part, got, far_in, near_in, ss, rs, h, g):
        pair_sum(part, got, rs, 2)
        pair_sum(part, got, rs, 1)
        send(part.at[y_far, c, pl.ds(0, h)], far_in.at[0, pl.ds(0, h)], ss.at[4], rs.at[4], ep, up)
        send(part.at[y_far, c, pl.ds(h, g - h)], far_in.at[1, pl.ds(0, g - h)], ss.at[5], rs.at[5], ep, dn)
        pair_sum(part, got, rs, 3)
        send(part.at[y_up, c, pl.ds(h, g - h)], near_in.at[0, pl.ds(h, g - h)], ss.at[6], rs.at[6], ep, up)
        pair_sum(part, got, rs, 0)
        send(part.at[y_dn, c, pl.ds(0, h)], near_in.at[1, pl.ds(0, h)], ss.at[7], rs.at[7], ep, dn)

    def ring_second(part, far_in, near_in, ss, rs, h, g):
        low, high = pl.ds(0, h), pl.ds(h, g - h)
        arrived(far_in.at[0, pl.ds(0, h)], rs.at[4])
        part[y_up, c, low] = (part[y_up, c, low].astype(F32) + far_in[0, pl.ds(0, h)].astype(F32)).astype(BF16)
        arrived(far_in.at[1, pl.ds(0, g - h)], rs.at[5])
        part[y_dn, c, high] = (part[y_dn, c, high].astype(F32) + far_in[1, pl.ds(0, g - h)].astype(F32)).astype(BF16)
        send(part.at[y_up, c, low], near_in.at[0, low], ss.at[8], rs.at[8], ep, up)
        send(part.at[y_dn, c, high], near_in.at[1, high], ss.at[9], rs.at[9], ep, dn)

    def ring_end(part, near_in, rs, h, g):
        low, high = pl.ds(0, h), pl.ds(h, g - h)
        arrived(near_in.at[0, high], rs.at[6])
        arrived(near_in.at[1, low], rs.at[7])
        arrived(near_in.at[0, low], rs.at[8])
        arrived(near_in.at[1, high], rs.at[9])
        return part[y, c].astype(F32) + near_in[0].astype(F32) + near_in[1].astype(F32)

    f_rows = slot_groups * CAP

    def experts(k):
        def one(e, carry):
            gate = jnp.zeros((f_rows, eff), F32)
            up_pre = jnp.zeros((f_rows, eff), F32)
            rows = jnp.concatenate([xs[k, j, :, e].reshape(f_rows, f) for j in range(n_tp)], axis=1)
            gate = jnp.dot(rows, wg[e], preferred_element_type=F32)
            up_pre = jnp.dot(rows, wu[e], preferred_element_type=F32)
            hidden = (gate / (1.0 + jnp.exp(-gate)) * up_pre).astype(BF16)
            for j in range(n_tp):
                res = jnp.dot(hidden, wd[e, :, j * f : (j + 1) * f], preferred_element_type=F32).astype(BF16)
                p_ref[k, j // 2, j % 2, pl.ds(0, slot_groups), e] = res.reshape(slot_groups, CAP, f)
            return carry

        lax.fori_loop(0, 2, one, 0)
        pair_send(p_ref.at[k], pr.at[k], rs_s.at[k], rs_r.at[k], (2, 1, 3, 0))

    def rs_first(k):
        ring_first(p_ref.at[k], pr.at[k], r2.at[k], r1.at[k], rs_s.at[k], rs_r.at[k], half, groups)

    def rs_second(k):
        ring_second(p_ref.at[k], r2.at[k], r1.at[k], rs_s.at[k], rs_r.at[k], half, groups)

    def rs_end(k):
        total = ring_end(p_ref.at[k], r1.at[k], rs_r.at[k], half, groups)
        y_ref[k] = total[:slot_groups].astype(BF16)
        shr[pl.ds(k * s_rows, s_rows)] = total[slot_groups:].reshape(s_rows, f)
        if k == 0:
            ret[z, x] = y_ref[0, x]
        for q in range(2):
            src_z = (z + nz + order[2 * k + q]) % nz
            for i in range(nx):
                if k == 0 and q == 0 and i == 0:
                    continue
                xx = (x + i) % nx
                pltpu.make_async_remote_copy(
                    src_ref=y_ref.at[k, q * nx + xx], dst_ref=ret.at[z, x], send_sem=rt_s, recv_sem=rt_r.at[k],
                    device_id=(src_z * nx + xx, tp), device_id_type=MESH,
                ).start()

    def combine(k):
        first = 1 if k == 0 else 0
        arrived(y_ref.at[k, pl.ds(0, slot_groups - first)], rt_r.at[k])
        total = jnp.zeros((t2, f), F32)
        for q in range(2):
            from_z = (z + nz - order[2 * k + q]) % nz
            rows = ret[from_z].reshape(per_z, f)
            total += jnp.dot(comb[from_z, 0], rows, preferred_element_type=F32)
            total += jnp.dot(comb[from_z, 1], rows, preferred_element_type=F32)
        if k == 0:
            acc[...] = total
        else:
            acc[...] += total

    def shared():
        for i in (14, 15, 16):
            loads[i].wait()
        rows = jnp.concatenate([n2[j] for j in range(n_tp)], axis=1)
        gate = jnp.dot(rows, sg[...], preferred_element_type=F32)
        up_pre = jnp.dot(rows, su[...], preferred_element_type=F32)
        hidden = (gate / (1.0 + jnp.exp(-gate)) * up_pre).astype(BF16)
        for j in range(n_tp):
            res = jnp.dot(hidden, sd[:, j * f : (j + 1) * f], preferred_element_type=F32).astype(BF16)
            res = res.reshape(chunks, groups - slot_groups, 2, CAP, f)
            for k in range(chunks):
                p_ref[k, j // 2, j % 2, pl.ds(slot_groups, groups - slot_groups)] = res[k]

    blk = BAND
    n_blk = t1 // blk
    lane_b = lax.broadcasted_iota(jnp.int32, (blk, 128), 1)
    low_half = (lane_b % HEAD) < HEAD // 2
    is_key = lane_b < HEAD

    def project(i, carry):
        b = (i + n_blk - 1) % n_blk
        start = pl.multiple_of(b * blk, blk)

        def norm(r, inner):
            at = pl.ds(pl.multiple_of(r * 32, 32), 32)
            rows = tok1[pl.ds(pl.multiple_of(start + r * 32, 32), 32)].astype(F32)
            scl = lax.rsqrt(jnp.mean(rows * rows, axis=-1, keepdims=True) + EPS)
            nrm[at] = (rows * scl * gain1[...]).astype(BF16)
            return inner

        lax.fori_loop(0, blk // 32, norm, 0)
        at = pl.ds(start, blk)
        ca, sa = cosa[pl.ds(ep, 1)], sina[pl.ds(ep, 1)]
        cb, sb = cosb[at], sinb[at]
        cosine = ca * cb - sa * sb
        sine = sa * cb + ca * sb
        sine = jnp.where(low_half, -sine, sine)

        def turn(v, co, si):
            other = jnp.where(low_half, pltpu.roll(v, 128 - HEAD // 2, 1), pltpu.roll(v, HEAD // 2, 1))
            return v * co + other * si

        rows = nrm[...]
        qv = jnp.dot(rows, wq[...], preferred_element_type=F32)
        qs[at] = turn(qv, cosine, sine).astype(BF16)
        kvv = jnp.dot(rows, wkv[...], preferred_element_type=F32)
        kv[pl.ds(pl.multiple_of(start + blk, blk), blk)] = turn(
            kvv, jnp.where(is_key, cosine, 1.0), jnp.where(is_key, sine, 0.0)
        ).astype(BF16)
        return carry

    def attend(b):
        keys = kv[pl.ds(b * blk, 2 * blk)]
        qb = qs[pl.ds(b * blk, blk)]
        zero = jnp.zeros_like(qb)
        q0 = jnp.where(is_key, qb, zero)
        q1 = jnp.where(is_key, pltpu.roll(qb.astype(F32), HEAD, 1).astype(BF16), zero)
        q_pos = lax.broadcasted_iota(jnp.int32, (blk, 2 * blk), 0) + blk
        k_pos = lax.broadcasted_iota(jnp.int32, (blk, 2 * blk), 1)
        gap = q_pos - k_pos
        seen = (gap >= 0) & (gap < BAND) & (k_pos + (ep * t1 + (b - 1) * blk) >= 0)
        outs = []
        for h, qh in enumerate((q0, q1)):
            s = lax.dot_general(qh, keys, (((1,), (1,)), ((), ())), preferred_element_type=F32) * HEAD**-0.5
            s = jnp.where(seen, s, -1e30)
            snk = sink[0:1, h : h + 1]
            peak = jnp.maximum(jnp.max(s, axis=-1, keepdims=True), snk)
            ex = jnp.where(seen, jnp.exp(s - peak), 0.0)
            den = jnp.sum(ex, axis=-1, keepdims=True) + jnp.exp(snk - peak)
            w = (ex / den).astype(BF16)
            outs.append(jnp.dot(w, keys, preferred_element_type=F32))
        att = jnp.where(is_key, pltpu.roll(outs[0], HEAD, 1), outs[1]).astype(BF16)
        res = jnp.dot(att, wo[...], preferred_element_type=F32).astype(BF16)
        pm[b] = res.reshape(pm.shape[1:])

    g_m = pm.shape[2]
    h_m = g_m // 2

    for i in (0, 1, 2, 3, 4, 5, 17, 18, 19, 20):
        loads[i].wait()
    wkv[...] = jnp.concatenate([wk[...], wv[...]], axis=1)
    project(0, 0)
    nxt = (ep + 1) % n_ep
    send(kv.at[pl.ds(t1, blk)], kv.at[pl.ds(0, blk)], halo_s, halo_r, nxt, tp)
    lax.fori_loop(1, n_blk, project, 0)
    gather_start(0)
    loads[6].wait()

    def attend_rest(b, carry):
        attend(b)
        return carry

    lax.fori_loop(1, n_blk, attend_rest, 0)
    gather_start(1)
    arrived(kv.at[pl.ds(0, blk)], halo_r)
    attend(0)
    pair_send(pm, pmr, mx_s, mx_r, (2, 1, 3, 0))
    gather_forward(0)
    shared()
    if chunks > 2:
        gather_start(2)
    gather_far(0)
    ring_first(pm, pmr, r2m, r1m, mx_s, mx_r, h_m, g_m)
    gather_forward(1)
    for k in range(3, chunks):
        gather_start(k)
    for i in (11, 12, 13):
        loads[i].wait()
    gather_end(0)
    experts(0)
    gather_far(1)
    ring_second(pm, r2m, r1m, mx_s, mx_r, h_m, g_m)

    def mixer_end():
        total = ring_end(pm, r1m, mx_r, h_m, g_m)
        mix_o[...] = total.astype(BF16).reshape(mix_o.shape)
        store = pltpu.make_async_copy(mix_o, mix_h, st_sem.at[0])
        store.start()
        return store

    store_mix = None
    for k in range(1, chunks):
        if k + 1 < chunks:
            gather_forward(k + 1)
        rs_first(k - 1)
        gather_end(k)
        experts(k)
        if k + 1 < chunks:
            gather_far(k + 1)
        if k == 1:
            store_mix = mixer_end()
        rs_second(k - 1)
        if k >= 2:
            rs_end(k - 2)
    rs_first(chunks - 1)
    if chunks >= 2:
        rs_end(chunks - 2)
    rs_second(chunks - 1)
    for k in range(chunks - 1):
        combine(k)
    rs_end(chunks - 1)
    combine(chunks - 1)
    moe_o[...] = (acc[...] + shr[...]).astype(BF16)
    store_moe = pltpu.make_async_copy(moe_o, moe_h, st_sem.at[1])
    store_moe.start()
    for src, sem in sends:
        pltpu.make_async_copy(src, src, sem).wait()
    whole = outgoing.at[pl.ds(0, n_ep - 1)]
    pltpu.make_async_copy(whole, whole, dsp_s).wait()
    pltpu.make_async_copy(whole, whole, rt_s).wait()
    store_mix.wait()
    store_moe.wait()


def build(mesh, nx=NX):
    n_ep = mesh.shape["ep"]
    n_tp = mesh.shape["tp"]
    nz = n_ep // nx

    def local(tok1, gain1, wq, wk, wv, sink, wo, tok2, gain2, routes, rw, wg, wu, wd, sg, su, sd):
        t1, d_model = tok1.shape
        t2, topk = routes.shape
        eff = wg.shape[2]
        sff = sg.shape[1]
        f = d_model // n_tp
        chunks = nz // 2
        slot_groups = 2 * nx
        s_groups = t2 // chunks // (2 * CAP)
        groups = slot_groups + s_groups
        half = (groups + 1) // 2
        rows_tp = t1 // n_tp
        tables = tuple(jnp.asarray(t) for t in rope_tables(t1, n_ep))
        args = (
            tok1, gain1.reshape(1, -1), wq, wk, wv, sink.reshape(1, -1), wo, tok2, gain2.reshape(1, -1), routes, rw,
            wg, wu, wd, sg, su, sd, *tables,
        )
        vm = pltpu.VMEM
        dma = pltpu.SemaphoreType.DMA
        g_m = rows_tp // 16
        scratch = [vm(a.shape, a.dtype) for a in args] + [
            vm((n_tp, t2, f), BF16),
            vm((8, 128), BF16),
            vm((nz, 2, t2, 2 * nx * CAP), BF16),
            vm((n_ep, 2, CAP, f), BF16),
            vm((chunks, n_tp, slot_groups, 2, CAP, f), BF16),
            vm((BAND, d_model), BF16),
            vm((t1, 128), BF16),
            vm((t1 + BAND, 128), BF16),
            vm((d_model, 128), BF16),
            vm((NY, 2, g_m, 16, d_model), BF16),
            vm((NY, g_m, 16, d_model), BF16),
            vm((2, g_m // 2, 16, d_model), BF16),
            vm((2, g_m, 16, d_model), BF16),
            vm((chunks, NY, 2, groups, 2, CAP, f), BF16),
            vm((chunks, NY, groups, 2, CAP, f), BF16),
            vm((chunks, 2, half, 2, CAP, f), BF16),
            vm((chunks, 2, groups, 2, CAP, f), BF16),
            vm((chunks, slot_groups, 2, CAP, f), BF16),
            vm((nz, nx, 2, CAP, f), BF16),
            vm((t2, f), F32),
            vm((t2, f), F32),
            vm((rows_tp, d_model), BF16),
            vm((t2, f), BF16),
            dma((len(args),)),
            dma, dma,
            dma, dma((chunks,)),
            dma((chunks, 9)), dma((chunks, 9)),
            dma((chunks, 10)), dma((chunks, 10)),
            dma((10,)), dma((10,)),
            dma, dma((chunks,)),
            dma((2,)),
        ]
        cfg = (nz, nx, n_tp, d_model, t1, t2, topk, eff, sff)
        return pl.pallas_call(
            functools.partial(kernel, cfg),
            name="whole",
            out_shape=(
                jax.ShapeDtypeStruct((rows_tp, d_model), BF16),
                jax.ShapeDtypeStruct((t2, f), BF16),
            ),
            in_specs=[pl.BlockSpec(memory_space=pl.ANY)] * len(args),
            out_specs=(pl.BlockSpec(memory_space=pl.ANY),) * 2,
            scratch_shapes=scratch,
            compiler_params=pltpu.CompilerParams(
                collective_id=0, has_side_effects=True, vmem_limit_bytes=60 * 1024 * 1024
            ),
        )(*args)

    in_specs = (
        P("ep", None), P(), P(None, "tp"), P(None, "tp"), P(None, "tp"), P("tp"), P("tp", None),
        P("ep", None), P(), P("ep", None), P("ep", None),
        P("ep", None, "tp"), P("ep", None, "tp"), P("ep", "tp", None),
        P(None, "tp"), P(None, "tp"), P("tp", None),
    )
    out_specs = (P(("ep", "tp"), None), P("ep", "tp"))
    return jax.shard_map(local, mesh=mesh, in_specs=in_specs, out_specs=out_specs, check_vma=False)


def solution(mesh):
    return build(mesh)
```

time: 195 us -> 92.7 us (0.48)
  waiting for transfers between devices: 82 us -> 0 us
  Pallas kernels: 0 us -> 81.8 us
  blocking collectives: 28.3 us -> 0 us
  matrix products: 25.6 us -> 0 us
  starting transfers between devices: 20.7 us -> 0 us
  other arithmetic: 15.6 us -> 0 us
  between operations: 14.4 us -> 0.64 us
  local copies, waits for them, and re-layouts: 6.4 us -> 9.89 us
    pallas_call x0 -> x1, Pallas kernels: none -> 81.8 us  [local(): pl.pallas_call(functools.partial(kernel, cfg), name='whole', out_shape=(j...]
    reduce_scatter x1 -> x0, waiting for transfers between devices: 38.9 us -> none  [local(): lax.psum_scatter(jnp.concatenate([routed_term, shared_term], axis=1).asty...]
    all_gather x1 -> x0, waiting for transfers between devices: 32 us -> none  [local(): piece = lax.all_gather(arrived, 'tp', axis=1, tiled=True)]
    all_to_all x1 -> x0, blocking collectives: 28.3 us -> none  [local(): lax.all_to_all(outgoing, 'ep', split_axis=0, concat_axis=0, tiled=True)]
    dot_general x12 -> x0, matrix products: 25.6 us -> none  [the longest x1 7.5 us: local(): jnp.einsum('sjcf,jfd->dsjc', hidden, w_down_exp, preferred_element_type=j...]
    all_to_all x2 -> x0, starting transfers between devices: 14 us -> none  [the longest x1 9.63 us: local(): lax.all_to_all(routed_part, 'ep', split_axis=1, concat_axis=1, tiled=True)]
    all_to_all x2 -> x0, waiting for transfers between devices: 11 us -> none  [the longest x1 11 us: local(): lax.all_to_all(routed_part, 'ep', split_axis=1, concat_axis=1, tiled=True)]
    unnamed x19 -> x6, local copies, waits for them, and re-layouts: 1.43 us -> 9.89 us
  transfers between devices with their start and end apart: 6 -> 0, of which waited for: 3 -> 0; matrix products, arithmetic and copies ran while one was open for 10% -> 0% of each run, Pallas kernels for 0% -> 0%
where the time goes in v1:
time: 92.7 us; the launch traced here: 92.3 us
  Pallas kernels  81.8 us (88%)
  local copies, waits for them, and re-layouts  9.89 us (11%)
    pallas_call x1, Pallas kernels, local(): pl.pallas_call(functools.partial(kernel, cfg), name='whole', out_shape=(j...  81.8 us
    unnamed x6, local copies, waits for them, and re-layouts  9.89 us

profile of v1, /device:TPU:2, one launch (start us, length us, event | category | flops | bytes accessed | tf_op | source)
XLA Modules:
  0.0 92.3 jit_solution(3491647332198322982)
XLA Ops:
  0.6 1.4 %copy.25.refs_9_ = s32[128,4]{1,0:T(8,128)} copy(s32[128,4]{0,1:T(4,128)} %param.30) | data formatting | bytes 4096 | tf_op args[9]
  2.0 1.4 %copy.26.refs_10_ = f32[128,4]{1,0:T(8,128)} copy(f32[128,4]{0,1:T(4,128)} %param.31) | data formatting | bytes 4096 | tf_op args[10]
  3.5 1.9 %copy.23.refs_3_ = bf16[2048,64]{1,0:T(8,128)(2,1)} copy(bf16[2048,64]{0,1:T(8,128)(2,1)} %param.24) | data formatting | bytes 524288 | tf_op args[3]
  5.4 2.0 %copy.24.refs_4_ = bf16[2048,64]{1,0:T(8,128)(2,1)} copy(bf16[2048,64]{0,1:T(8,128)(2,1)} %param.25) | data formatting | bytes 524288 | tf_op args[4]
  7.4 81.8 %whole.1 = (bf16[64,2048]{1,0:T(8,128)(2,1)}, bf16[128,256]{1,0:T(8,128)(2,1)}) custom-call(bf16[512,2048]{1,0:T(8,128)(2,1)} %refs_0_.1, f32[1,2048]{1,0:T(1,128)} %bitcast.3, bf16[2048,128]{1,0:T(8,128)(2,1)} %refs_2_.1, bf16[2048,64]{1,0:T(8,128)(2,1)} %copy.23.refs_3_, bf16[2048,64]{1,0:T(8,128)(2,1)} %copy.24.refs_4_, f32[1,2]{1,0:T(1,128)} %bitcast.5, ...), custom_call_target="tpu_custom_call" | custom-call | tf_op jit(solution)/shard_map/whole/pallas_call | solution.py:501
  89.2 1.7 %copy.29 = bf16[64,2048]{1,0:T(8,128)(2,1)} copy(bf16[64,2048]{1,0:T(8,128)(2,1)} %get-tuple-element.4) | data formatting | bytes 524288
  90.9 1.5 %copy.30 = bf16[128,256]{1,0:T(8,128)(2,1)} copy(bf16[128,256]{1,0:T(8,128)(2,1)} %get-tuple-element.5) | data formatting | bytes 131072

commit v2 on v1

v2 whole, which is shorter than its diff:
```python
import functools

import jax
import jax.numpy as jnp
import numpy as np
from jax import lax
from jax.experimental import pallas as pl
from jax.experimental.pallas import tpu as pltpu
from jax.sharding import PartitionSpec as P

HEAD = 64
BAND = 128
CAP = 16
NX = 4
NY = 4
ROPE_BASE = 10000.0
EPS = 1e-06
MESH = pl.DeviceIdType.MESH
F32 = jnp.float32
BF16 = jnp.bfloat16


CHUNK_Z = ((0, 1), (4, -2), (3, -3), (2,), (-1,))
SHARED = (2, 2, 0, 0, 0)
FAR_DIRECT = (0,)
SEND_ORDER = ((0, 0), (0, 1), (1, 0), (2, 0), (3, 0), (4, 0))


def rope_tables(rows, n_ep):
    freqs = ROPE_BASE ** (-np.arange(0, HEAD, 2, dtype=np.float64) / HEAD)
    lanes = np.tile(freqs, 4)[None, :]
    within = np.arange(rows, dtype=np.float64)[:, None] * lanes
    starts = np.arange(n_ep, dtype=np.float64)[:, None] * rows * lanes
    return tuple(
        np.asarray(t, np.float32) for t in (np.cos(within), np.sin(within), np.cos(starts), np.sin(starts))
    )


def kernel(cfg, *refs):
    nz, nx, n_tp, d_model, t1, t2, topk, eff, sff = cfg
    n_in = 21
    (
        tok1_h, gain1_h, wq_h, wk_h, wv_h, sink_h, wo_h, tok2_h, gain2_h, routes_h, rw_h,
        wg_h, wu_h, wd_h, sg_h, su_h, sd_h, cosb_h, sinb_h, cosa_h, sina_h,
    ) = refs[:n_in]
    mix_h, moe_h = refs[n_in : n_in + 2]
    (
        tok1, gain1, wq, wk, wv, sink, wo, tok2, gain2, routes, rw,
        wg, wu, wd, sg, su, sd, cosb, sinb, cosa, sina,
    ) = refs[n_in + 2 : 2 * n_in + 2]
    (
        n2, comb, outgoing, xs, nrm, qs, kv, wkv, wof, att, attx, p_ref, pr, r2, r1, y_ref, ret, shr,
        acc, mix_o, moe_o,
        load_sem, halo_s, halo_r, dsp_s, dsp_r, ag_s, ag_r, rs_s, rs_r, wo_s, wo_r, at_s, at_r, rt_s, rt_r, st_sem,
    ) = refs[2 * n_in + 2 :]
    f = d_model // n_tp
    n_ep = nz * nx
    chunks = len(CHUNK_Z)
    slots_of = [nx * len(c) for c in CHUNK_Z]
    groups_of = [a + b for a, b in zip(slots_of, SHARED)]
    half_of = [g // 2 for g in groups_of]
    piece = 2 * CAP
    shared_at = [piece * sum(SHARED[:k]) for k in range(chunks)]

    ep = lax.axis_index("ep")
    tp = lax.axis_index("tp")
    z, x = ep // nx, ep % nx
    y, c = tp // 2, tp % 2
    partner = y * 2 + (1 - c)
    y_up, y_dn, y_far = (y + 1) % NY, (y + NY - 1) % NY, (y + 2) % NY
    up, dn, far = y_up * 2 + c, y_dn * 2 + c, y_far * 2 + c

    hbm = (tok1_h, gain1_h, wq_h, wk_h, wv_h, sink_h, wo_h, tok2_h, gain2_h, routes_h, rw_h,
           wg_h, wu_h, wd_h, sg_h, su_h, sd_h, cosb_h, sinb_h, cosa_h, sina_h)
    vmem = (tok1, gain1, wq, wk, wv, sink, wo, tok2, gain2, routes, rw,
            wg, wu, wd, sg, su, sd, cosb, sinb, cosa, sina)
    vmem = vmem[:3] + (wkv.at[pl.ds(0, HEAD)], wkv.at[pl.ds(HEAD, HEAD)]) + vmem[5:]
    loads = [pltpu.make_async_copy(h, v, load_sem.at[i]) for i, (h, v) in enumerate(zip(hbm, vmem))]
    for i in (7, 8, 9, 10, 0, 1, 2, 3, 4, 5, 17, 18, 19, 20, 6, 14, 15, 16, 11, 12, 13):
        loads[i].start()

    barrier = pltpu.get_barrier_semaphore()
    for dz in range(nz):
        for dx in range(nx):
            if dz or dx:
                peer = ((z + dz) % nz) * nx + (x + dx) % nx
                pl.semaphore_signal(barrier, inc=1, device_id=(peer, tp), device_id_type=MESH)
    for step in range(1, n_tp):
        pl.semaphore_signal(barrier, inc=1, device_id=(ep, (tp + step) % n_tp), device_id_type=MESH)

    sends = []

    def send(src, dst, ssem, rsem, to_ep, to_tp):
        copy = pltpu.make_async_remote_copy(
            src_ref=src, dst_ref=dst, send_sem=ssem, recv_sem=rsem, device_id=(to_ep, to_tp), device_id_type=MESH
        )
        copy.start()
        sends.append((src, ssem))

    def arrived(dst, rsem):
        pltpu.make_async_copy(dst, dst, rsem).wait()

    with jax.named_scope("load_2"):
        for i in (7, 8, 9, 10):
            loads[i].wait()

    wide = tok2[...].astype(F32)
    scale = lax.rsqrt(jnp.mean(wide * wide, axis=-1, keepdims=True) + EPS)
    normed = (wide * scale * gain2[...]).astype(BF16)
    for j in range(n_tp):
        n2[j] = normed[:, j * f : (j + 1) * f]

    sub = lax.broadcasted_iota(jnp.int32, (128, t2), 0)
    named_t = jnp.zeros((128, t2), F32)
    weight_t = jnp.zeros((128, t2), F32)
    for k in range(topk):
        hit = sub == routes[k : k + 1]
        named_t = jnp.where(hit, 1.0, named_t)
        weight_t = jnp.where(hit, rw[k : k + 1], weight_t)
    row_i = lax.broadcasted_iota(jnp.int32, (t2, t2), 0)
    col_i = lax.broadcasted_iota(jnp.int32, (t2, t2), 1)
    before = jnp.where(row_i < col_i, 1.0, 0.0).astype(BF16)
    rank_t = jnp.dot(named_t.astype(BF16), before, preferred_element_type=F32)
    rank_t = jnp.where(named_t > 0.5, rank_t, -1.0)[: 2 * n_ep]
    cap_i = lax.broadcasted_iota(jnp.int32, (2 * n_ep, CAP, t2), 1).astype(F32)
    dispatch = jnp.where(rank_t[:, None, :] == cap_i, 1.0, 0.0).astype(BF16).reshape(2 * n_ep * CAP, t2)
    for far_one, column in enumerate((tp, far)):
        sent = jnp.dot(dispatch, n2[column], preferred_element_type=F32).astype(BF16)
        outgoing[far_one] = sent.reshape(n_ep, 2, CAP, f)

    def dispatch_all():
        with jax.named_scope("barrier"):
            pl.semaphore_wait(barrier, n_ep - 1 + n_tp - 1)
        send(kv.at[pl.ds(t1, BAND)], kv.at[pl.ds(0, BAND)], halo_s, halo_r, (ep + 1) % n_ep, tp)

        for far_one, column in enumerate((tp, far)):
            xs[0, column, x] = outgoing[far_one, ep]
        for k, far_one in SEND_ORDER:
            for q, dz in enumerate(CHUNK_Z[k]):
                to_z = (z + nz - dz) % nz
                for i in range(nx):
                    if dz == 0 and i == 0:
                        continue
                    to = to_z * nx + (x + i) % nx
                    pltpu.make_async_remote_copy(
                        src_ref=outgoing.at[far_one, to], dst_ref=xs.at[k, (tp, far)[far_one], q * nx + x],
                        send_sem=dsp_s, recv_sem=dsp_r.at[k, far_one], device_id=(to, tp),
                        device_id_type=MESH,
                    ).start()

    per_z = 2 * nx * CAP

    def combine_weights():
        after = jnp.where(row_i > col_i, 1.0, 0.0).astype(BF16)
        named, weight = named_t.T, weight_t.T
        rank = jnp.dot(after, named.astype(BF16), preferred_element_type=F32)
        rank = jnp.where(named > 0.5, rank, -1.0).astype(BF16)
        w_hi = weight.astype(BF16)
        w_lo = (weight - w_hi.astype(F32)).astype(BF16)
        for zz in range(nz):
            e_row = lax.broadcasted_iota(jnp.int32, (128, per_z), 0)
            e_col = lax.broadcasted_iota(jnp.int32, (128, per_z), 1)
            spread = jnp.where(e_row == zz * 2 * nx + e_col // CAP, 1.0, 0.0).astype(BF16)
            slot = (lax.broadcasted_iota(jnp.int32, (t2, per_z), 1) % CAP).astype(F32)
            mine = jnp.dot(rank, spread, preferred_element_type=F32) == slot
            comb[zz, 0] = jnp.where(mine, jnp.dot(w_hi, spread, preferred_element_type=F32), 0.0).astype(BF16)
            comb[zz, 1] = jnp.where(mine, jnp.dot(w_lo, spread, preferred_element_type=F32), 0.0).astype(BF16)

    def halves(k):
        return pl.ds(0, slots_of[k] // 2), pl.ds(slots_of[k] // 2, slots_of[k] // 2)

    def dispatched(k, far_one):
        first = 1 if k == 0 else 0
        arrived(xs.at[k, 0, pl.ds(0, slots_of[k] - first)], dsp_r.at[k, far_one])

    def gather_start(k):
        dispatched(k, 0)
        own = xs.at[k, tp, pl.ds(0, slots_of[k])]
        send(own, own, ag_s.at[k, 0], ag_r.at[k, 0], ep, up)
        send(own, own, ag_s.at[k, 1], ag_r.at[k, 1], ep, dn)
        send(own, own, ag_s.at[k, 2], ag_r.at[k, 2], ep, partner)

    def gather_forward(k):
        low, high = halves(k)
        whole = pl.ds(0, slots_of[k])
        for i, (side, part, to) in enumerate(((dn, low, up), (up, high, dn))):
            got = xs.at[k, side, whole]
            arrived(got, ag_r.at[k, i])
            if k not in FAR_DIRECT:
                on = xs.at[k, side, part]
                send(on, on, ag_s.at[k, 3 + i], ag_r.at[k, 3 + i], ep, to)
            send(got, got, ag_s.at[k, 5 + i], ag_r.at[k, 5 + i], ep, partner)

    def gather_far(k):
        if k in FAR_DIRECT:
            dispatched(k, 1)
            got = xs.at[k, far, pl.ds(0, slots_of[k])]
            send(got, got, ag_s.at[k, 7], ag_r.at[k, 7], ep, partner)
            return
        for i, part in enumerate(halves(k)):
            got = xs.at[k, far, part]
            arrived(got, ag_r.at[k, 3 + i])
            send(got, got, ag_s.at[k, 7 + i], ag_r.at[k, 7 + i], ep, partner)

    def gather_end(k):
        other = 1 - c
        whole = pl.ds(0, slots_of[k])
        arrived(xs.at[k, partner, whole], ag_r.at[k, 2])
        arrived(xs.at[k, y_dn * 2 + other, whole], ag_r.at[k, 5])
        arrived(xs.at[k, y_up * 2 + other, whole], ag_r.at[k, 6])
        if k in FAR_DIRECT:
            arrived(xs.at[k, y_far * 2 + other, whole], ag_r.at[k, 7])
            return
        for i, part in enumerate(halves(k)):
            arrived(xs.at[k, y_far * 2 + other, part], ag_r.at[k, 7 + i])

    def pair_send(part, got, ss, rs, g):
        for o in (2, 1, 3, 0):
            t = (y + o) % NY
            send(part.at[t, 1 - c, pl.ds(0, g)], got.at[t, pl.ds(0, g)], ss.at[o], rs.at[o], ep, partner)

    def pair_sum(part, got, rs, o, g):
        t = (y + o) % NY
        at = pl.ds(0, g)
        arrived(got.at[t, at], rs.at[o])
        part[t, c, at] = (part[t, c, at].astype(F32) + got[t, at].astype(F32)).astype(BF16)

    def ring_first(part, got, far_in, near_in, ss, rs, h, g):
        pair_sum(part, got, rs, 2, g)
        pair_sum(part, got, rs, 1, g)
        send(part.at[y_far, c, pl.ds(0, h)], far_in.at[0, pl.ds(0, h)], ss.at[4], rs.at[4], ep, up)
        send(part.at[y_far, c, pl.ds(h, g - h)], far_in.at[1, pl.ds(0, g - h)], ss.at[5], rs.at[5], ep, dn)
        pair_sum(part, got, rs, 3, g)
        send(part.at[y_up, c, pl.ds(h, g - h)], near_in.at[0, pl.ds(h, g - h)], ss.at[6], rs.at[6], ep, up)
        pair_sum(part, got, rs, 0, g)
        send(part.at[y_dn, c, pl.ds(0, h)], near_in.at[1, pl.ds(0, h)], ss.at[7], rs.at[7], ep, dn)

    def ring_second(part, far_in, near_in, ss, rs, h, g):
        low, high = pl.ds(0, h), pl.ds(h, g - h)
        arrived(far_in.at[0, pl.ds(0, h)], rs.at[4])
        part[y_up, c, low] = (part[y_up, c, low].astype(F32) + far_in[0, pl.ds(0, h)].astype(F32)).astype(BF16)
        arrived(far_in.at[1, pl.ds(0, g - h)], rs.at[5])
        part[y_dn, c, high] = (part[y_dn, c, high].astype(F32) + far_in[1, pl.ds(0, g - h)].astype(F32)).astype(BF16)
        send(part.at[y_up, c, low], near_in.at[0, low], ss.at[8], rs.at[8], ep, up)
        send(part.at[y_dn, c, high], near_in.at[1, high], ss.at[9], rs.at[9], ep, dn)

    def ring_end(part, near_in, rs, h, g):
        low, high = pl.ds(0, h), pl.ds(h, g - h)
        arrived(near_in.at[0, high], rs.at[6])
        arrived(near_in.at[1, low], rs.at[7])
        arrived(near_in.at[0, low], rs.at[8])
        arrived(near_in.at[1, high], rs.at[9])
        at = pl.ds(0, g)
        return part[y, c, at].astype(F32) + near_in[0, at].astype(F32) + near_in[1, at].astype(F32)

    def experts(k):
        n_slots = slots_of[k]
        at = pl.ds(0, n_slots)

        def one(e, carry):
            rows = jnp.concatenate([xs[k, j, at, e].reshape(n_slots * CAP, f) for j in range(n_tp)], axis=1)
            gate = jnp.dot(rows, wg[e], preferred_element_type=F32)
            up_pre = jnp.dot(rows, wu[e], preferred_element_type=F32)
            hidden = (gate / (1.0 + jnp.exp(-gate)) * up_pre).astype(BF16)
            for j in range(n_tp):
                res = jnp.dot(hidden, wd[e, :, j * f : (j + 1) * f], preferred_element_type=F32).astype(BF16)
                p_ref[k, j // 2, j % 2, at, e] = res.reshape(n_slots, CAP, f)
            return carry

        lax.fori_loop(0, 2, one, 0)
        pair_send(p_ref.at[k], pr.at[k], rs_s.at[k], rs_r.at[k], groups_of[k])

    def rs_first(k):
        ring_first(p_ref.at[k], pr.at[k], r2.at[k], r1.at[k], rs_s.at[k], rs_r.at[k], half_of[k], groups_of[k])

    def rs_second(k):
        ring_second(p_ref.at[k], r2.at[k], r1.at[k], rs_s.at[k], rs_r.at[k], half_of[k], groups_of[k])

    def rs_end(k):
        total = ring_end(p_ref.at[k], r1.at[k], rs_r.at[k], half_of[k], groups_of[k])
        n_slots = slots_of[k]
        y_ref[k, pl.ds(0, n_slots)] = total[:n_slots].astype(BF16)
        if SHARED[k]:
            shr[pl.ds(shared_at[k], SHARED[k] * piece)] = total[n_slots:].reshape(SHARED[k] * piece, f)
        if k == 0:
            ret[z, x] = y_ref[0, x]
        for q, dz in enumerate(CHUNK_Z[k]):
            src_z = (z + nz + dz) % nz
            for i in range(nx):
                if dz == 0 and i == 0:
                    continue
                xx = (x + i) % nx
                pltpu.make_async_remote_copy(
                    src_ref=y_ref.at[k, q * nx + xx], dst_ref=ret.at[z, x], send_sem=rt_s, recv_sem=rt_r.at[k],
                    device_id=(src_z * nx + xx, tp), device_id_type=MESH,
                ).start()

    def combine(k):
        first = 1 if k == 0 else 0
        arrived(y_ref.at[k, pl.ds(0, slots_of[k] - first)], rt_r.at[k])
        total = jnp.zeros((t2, f), F32)
        for dz in CHUNK_Z[k]:
            from_z = (z + nz - dz) % nz
            rows = ret[from_z].reshape(per_z, f)
            total += jnp.dot(comb[from_z, 0], rows, preferred_element_type=F32)
            total += jnp.dot(comb[from_z, 1], rows, preferred_element_type=F32)
        if k == 0:
            acc[...] = total
        else:
            acc[...] += total

    def shared():
        for i in (14, 15, 16):
            loads[i].wait()
        rows = jnp.concatenate([n2[j] for j in range(n_tp)], axis=1)
        gate = jnp.dot(rows, sg[...], preferred_element_type=F32)
        up_pre = jnp.dot(rows, su[...], preferred_element_type=F32)
        hidden = (gate / (1.0 + jnp.exp(-gate)) * up_pre).astype(BF16)
        for j in range(n_tp):
            res = jnp.dot(hidden, sd[:, j * f : (j + 1) * f], preferred_element_type=F32).astype(BF16)
            for k in range(chunks):
                if SHARED[k]:
                    rows_k = res[shared_at[k] : shared_at[k] + SHARED[k] * piece]
                    p_ref[k, j // 2, j % 2, pl.ds(slots_of[k], SHARED[k])] = rows_k.reshape(SHARED[k], 2, CAP, f)

    blk = BAND
    n_blk = t1 // blk
    lane_b = lax.broadcasted_iota(jnp.int32, (blk, 128), 1)
    low_half = (lane_b % HEAD) < HEAD // 2
    is_key = lane_b < HEAD

    def project(i, carry):
        b = (i + n_blk - 1) % n_blk
        start = pl.multiple_of(b * blk, blk)

        def norm(r, inner):
            at = pl.ds(pl.multiple_of(r * 32, 32), 32)
            rows = tok1[pl.ds(pl.multiple_of(start + r * 32, 32), 32)].astype(F32)
            scl = lax.rsqrt(jnp.mean(rows * rows, axis=-1, keepdims=True) + EPS)
            nrm[at] = (rows * scl * gain1[...]).astype(BF16)
            return inner

        lax.fori_loop(0, blk // 32, norm, 0)
        at = pl.ds(start, blk)
        ca, sa = cosa[pl.ds(ep, 1)], sina[pl.ds(ep, 1)]
        cb, sb = cosb[at], sinb[at]
        cosine = ca * cb - sa * sb
        sine = sa * cb + ca * sb
        sine = jnp.where(low_half, -sine, sine)

        def turn(v, co, si):
            other = jnp.where(low_half, pltpu.roll(v, 128 - HEAD // 2, 1), pltpu.roll(v, HEAD // 2, 1))
            return v * co + other * si

        rows = nrm[...]
        qv = jnp.dot(rows, wq[...], preferred_element_type=F32)
        qs[at] = turn(qv, cosine, sine).astype(BF16)
        kvv = lax.dot_general(rows, wkv[...], (((1,), (1,)), ((), ())), preferred_element_type=F32)
        kv[pl.ds(pl.multiple_of(start + blk, blk), blk)] = turn(
            kvv, jnp.where(is_key, cosine, 1.0), jnp.where(is_key, sine, 0.0)
        ).astype(BF16)
        return carry

    def attend(b):
        keys = kv[pl.ds(b * blk, 2 * blk)]
        qb = qs[pl.ds(b * blk, blk)]
        zero = jnp.zeros_like(qb)
        q0 = jnp.where(is_key, qb, zero)
        q1 = jnp.where(is_key, pltpu.roll(qb.astype(F32), HEAD, 1).astype(BF16), zero)
        q_pos = lax.broadcasted_iota(jnp.int32, (blk, 2 * blk), 0) + blk
        k_pos = lax.broadcasted_iota(jnp.int32, (blk, 2 * blk), 1)
        gap = q_pos - k_pos
        seen = (gap >= 0) & (gap < BAND) & (k_pos + (ep * t1 + (b - 1) * blk) >= 0)
        outs = []
        for h, qh in enumerate((q0, q1)):
            s = lax.dot_general(qh, keys, (((1,), (1,)), ((), ())), preferred_element_type=F32) * HEAD**-0.5
            s = jnp.where(seen, s, -1e30)
            snk = sink[0:1, h : h + 1]
            peak = jnp.maximum(jnp.max(s, axis=-1, keepdims=True), snk)
            ex = jnp.where(seen, jnp.exp(s - peak), 0.0)
            den = jnp.sum(ex, axis=-1, keepdims=True) + jnp.exp(snk - peak)
            w = (ex / den).astype(BF16)
            outs.append(jnp.dot(w, keys, preferred_element_type=F32))
        att[pl.ds(b * blk, blk)] = jnp.where(is_key, pltpu.roll(outs[0], HEAD, 1), outs[1]).astype(BF16)

    def stage(name, fn, *operands):
        with jax.named_scope(name):
            return fn(*operands)

    def wait_loads(*which):
        for i in which:
            loads[i].wait()

    def project_first():
        wait_loads(0, 1, 2, 3, 4, 5, 17, 18, 19, 20)
        lax.fori_loop(0, n_blk - 1, project, 0)

    def project_last():
        project(n_blk - 1, 0)

    def attend_rest(b, carry):
        attend(b)
        return carry

    def attend_later():
        lax.fori_loop(1, n_blk, attend_rest, 0)

    rows_tp = t1 // n_tp

    def attend_first():
        arrived(kv.at[pl.ds(0, blk)], halo_r)
        attend(0)
        for step in range(1, n_tp):
            to = (tp + step) % n_tp
            pltpu.make_async_remote_copy(
                src_ref=att.at[pl.ds(pl.multiple_of(to * rows_tp, rows_tp), rows_tp)], dst_ref=attx.at[tp],
                send_sem=at_s, recv_sem=at_r, device_id=(ep, to), device_id_type=MESH,
            ).start()
        attx[tp] = att[pl.ds(pl.multiple_of(tp * rows_tp, rows_tp), rows_tp)]

    x_up, x_dn, x_far = (x + 1) % nx, (x + nx - 1) % nx, (x + 2) % nx
    w_rows = 128 // nx
    w_half = w_rows // 2

    def weight_y_start():
        wait_loads(6)
        part = wo.at[pl.ds(pl.multiple_of(x * w_rows, w_rows), w_rows)]
        send(part, wof.at[x, c, y], wo_s.at[0], wo_r.at[0], ep, up)
        send(part, wof.at[x, c, y], wo_s.at[1], wo_r.at[1], ep, dn)
        wof[x, c, y] = wo[pl.ds(pl.multiple_of(x * w_rows, w_rows), w_rows)]

    def weight_y_forward():
        for i, (side, start, to) in enumerate(((y_dn, 0, up), (y_up, w_half, dn))):
            arrived(wof.at[x, c, side], wo_r.at[i])
            on = wof.at[x, c, side, pl.ds(start, w_half)]
            send(on, on, wo_s.at[2 + i], wo_r.at[2 + i], ep, to)

    def weight_x_start():
        for i, start in enumerate((0, w_half)):
            arrived(wof.at[x, c, y_far, pl.ds(start, w_half)], wo_r.at[2 + i])
        own = wof.at[x, c]
        send(own, own, wo_s.at[4], wo_r.at[4], z * nx + x_up, tp)
        send(own, own, wo_s.at[5], wo_r.at[5], z * nx + x_dn, tp)
        send(own, own, wo_s.at[8], wo_r.at[8], ep, partner)

    def weight_x_forward():
        for i, (side, start, to) in enumerate(((x_dn, 0, x_up), (x_up, NY // 2, x_dn))):
            got = wof.at[side, c]
            arrived(got, wo_r.at[4 + i])
            on = wof.at[side, c, pl.ds(start, NY // 2)]
            send(on, on, wo_s.at[6 + i], wo_r.at[6 + i], z * nx + to, tp)
            send(got, got, wo_s.at[9 + i], wo_r.at[9 + i], ep, partner)

    def weight_x_far():
        for i, start in enumerate((0, NY // 2)):
            got = wof.at[x_far, c, pl.ds(start, NY // 2)]
            arrived(got, wo_r.at[6 + i])
            send(got, got, wo_s.at[11 + i], wo_r.at[11 + i], ep, partner)

    def mixer_end():
        other = 1 - c
        arrived(wof.at[x, other], wo_r.at[8])
        arrived(wof.at[x_dn, other], wo_r.at[9])
        arrived(wof.at[x_up, other], wo_r.at[10])
        for i, start in enumerate((0, NY // 2)):
            arrived(wof.at[x_far, other, pl.ds(start, NY // 2)], wo_r.at[11 + i])
        arrived(attx.at[pl.ds(0, n_tp - 1)], at_r)
        rows = jnp.concatenate([attx[j] for j in range(n_tp)], axis=1)
        n_cols = 256

        def columns(n, carry):
            at = pl.ds(pl.multiple_of(n * n_cols, n_cols), n_cols)
            parts = [wof[q, j % 2, j // 2, :, at] for j in range(n_tp) for q in range(nx)]
            mix_o[:, at] = jnp.dot(rows, jnp.concatenate(parts, axis=0), preferred_element_type=F32).astype(BF16)
            return carry

        lax.fori_loop(0, d_model // n_cols, columns, 0)
        store = pltpu.make_async_copy(mix_o, mix_h, st_sem.at[0])
        store.start()
        return store

    stage("project", project_first)
    stage("dispatch", dispatch_all)
    stage("w_y_start", weight_y_start)
    stage("project_last", project_last)
    stage("attend", attend_later)
    stage("ag_start0", gather_start, 0)
    stage("w_y_fwd", weight_y_forward)
    stage("attend0", attend_first)
    stage("ag_start1", gather_start, 1)
    stage("ag_fwd0", gather_forward, 0)
    stage("shared", shared)
    stage("w_x_start", weight_x_start)
    stage("ag_far0", gather_far, 0)
    stage("ag_start2", gather_start, 2)
    stage("ag_fwd1", gather_forward, 1)
    stage("load_w", wait_loads, 11, 12, 13)
    stage("ag_end0", gather_end, 0)
    stage("experts0", experts, 0)
    stage("weights", combine_weights)
    stage("ag_start3", gather_start, 3)
    stage("ag_start4", gather_start, 4)
    stage("rs_first0", rs_first, 0)
    stage("ag_far1", gather_far, 1)
    store_mix = None
    for k in range(1, chunks):
        if k + 1 < chunks:
            stage(f"ag_fwd{k + 1}", gather_forward, k + 1)
        if k >= 2:
            stage(f"rs_first{k - 1}", rs_first, k - 1)
        stage(f"ag_end{k}", gather_end, k)
        stage(f"experts{k}", experts, k)
        if k + 1 < chunks:
            stage(f"ag_far{k + 1}", gather_far, k + 1)
        if k == 1:
            stage("w_x_fwd", weight_x_forward)
        if k == 2:
            stage("w_x_far", weight_x_far)
        stage(f"rs_second{k - 1}", rs_second, k - 1)
        if k == 3:
            store_mix = stage("mix_end", mixer_end)
        if k >= 2:
            stage(f"rs_end{k - 2}", rs_end, k - 2)
    last = chunks - 1
    stage(f"rs_first{last}", rs_first, last)
    stage(f"rs_end{last - 1}", rs_end, last - 1)
    stage(f"rs_second{last}", rs_second, last)
    stage("combine0", combine, 0)
    stage(f"rs_end{last}", rs_end, last)
    for k in range(1, chunks):
        stage(f"combine{k}", combine, k)

    def finish():
        moe_o[...] = (acc[...] + shr[...]).astype(BF16)
        store_moe = pltpu.make_async_copy(moe_o, moe_h, st_sem.at[1])
        store_moe.start()
        for src, sem in sends:
            pltpu.make_async_copy(src, src, sem).wait()
        whole = outgoing.at[0, pl.ds(0, n_ep - 1)]
        sent_far = sum(slots_of[k] for k in FAR_DIRECT) - (1 if 0 in FAR_DIRECT else 0)
        pltpu.make_async_copy(whole, whole, dsp_s).wait()
        if sent_far:
            far_part = outgoing.at[1, pl.ds(0, sent_far)]
            pltpu.make_async_copy(far_part, far_part, dsp_s).wait()
        pltpu.make_async_copy(whole, whole, rt_s).wait()
        rows_out = attx.at[pl.ds(0, n_tp - 1)]
        pltpu.make_async_copy(rows_out, rows_out, at_s).wait()
        store_mix.wait()
        store_moe.wait()

    stage("finish", finish)


def build(mesh, nx=NX):
    n_ep = mesh.shape["ep"]
    n_tp = mesh.shape["tp"]
    nz = n_ep // nx

    def local(tok1, gain1, wq, wk, wv, sink, wo, tok2, gain2, routes, rw, wg, wu, wd, sg, su, sd):
        t1, d_model = tok1.shape
        t2, topk = routes.shape
        eff = wg.shape[2]
        sff = sg.shape[1]
        f = d_model // n_tp
        chunks = len(CHUNK_Z)
        slot_groups = nx * max(len(c) for c in CHUNK_Z)
        groups = max(nx * len(c) + b for c, b in zip(CHUNK_Z, SHARED))
        half = (groups + 1) // 2
        rows_tp = t1 // n_tp
        tables = tuple(jnp.asarray(t) for t in rope_tables(t1, n_ep))
        args = (
            tok1, gain1.reshape(1, -1), wq, wk.T, wv.T, sink.reshape(1, -1), wo, tok2, gain2.reshape(1, -1), routes.T, rw.T,
            wg, wu, wd, sg, su, sd, *tables,
        )
        vm = pltpu.VMEM
        dma = pltpu.SemaphoreType.DMA
        scratch = [vm((8, 128) if i in (3, 4) else a.shape, a.dtype) for i, a in enumerate(args)] + [
            vm((n_tp, t2, f), BF16),
                vm((nz, 2, t2, 2 * nx * CAP), BF16),
            vm((2, n_ep, 2, CAP, f), BF16),
            vm((chunks, n_tp, slot_groups, 2, CAP, f), BF16),
            vm((BAND, d_model), BF16),
            vm((t1, 128), BF16),
            vm((t1 + BAND, 128), BF16),
            vm((128, d_model), BF16),
            vm((nx, 2, NY, 128 // nx, d_model), BF16),
            vm((t1, 128), BF16),
            vm((n_tp, rows_tp, 128), BF16),
            vm((chunks, NY, 2, groups, 2, CAP, f), BF16),
            vm((chunks, NY, groups, 2, CAP, f), BF16),
            vm((chunks, 2, half, 2, CAP, f), BF16),
            vm((chunks, 2, groups, 2, CAP, f), BF16),
            vm((chunks, slot_groups, 2, CAP, f), BF16),
            vm((nz, nx, 2, CAP, f), BF16),
            vm((t2, f), F32),
            vm((t2, f), F32),
            vm((rows_tp, d_model), BF16),
            vm((t2, f), BF16),
            dma((len(args),)),
            dma, dma,
            dma, dma((chunks, 2)),
            dma((chunks, 9)), dma((chunks, 9)),
            dma((chunks, 10)), dma((chunks, 10)),
            dma((13,)), dma((13,)),
            dma, dma,
            dma, dma((chunks,)),
            dma((2,)),
        ]
        cfg = (nz, nx, n_tp, d_model, t1, t2, topk, eff, sff)
        return pl.pallas_call(
            functools.partial(kernel, cfg),
            name="whole",
            out_shape=(
                jax.ShapeDtypeStruct((rows_tp, d_model), BF16),
                jax.ShapeDtypeStruct((t2, f), BF16),
            ),
            in_specs=[pl.BlockSpec(memory_space=pl.ANY)] * len(args),
            out_specs=(pl.BlockSpec(memory_space=pl.ANY),) * 2,
            scratch_shapes=scratch,
            compiler_params=pltpu.CompilerParams(
                collective_id=0, has_side_effects=True, vmem_limit_bytes=60 * 1024 * 1024
            ),
        )(*args)

    in_specs = (
        P("ep", None), P(), P(None, "tp"), P(None, "tp"), P(None, "tp"), P("tp"), P("tp", None),
        P("ep", None), P(), P("ep", None), P("ep", None),
        P("ep", None, "tp"), P("ep", None, "tp"), P("ep", "tp", None),
        P(None, "tp"), P(None, "tp"), P("tp", None),
    )
    out_specs = (P(("ep", "tp"), None), P("ep", "tp"))
    return jax.shard_map(local, mesh=mesh, in_specs=in_specs, out_specs=out_specs, check_vma=False)


def solution(mesh):
    return build(mesh)
```

time: 92.7 us -> 77.8 us (0.84)
  Pallas kernels: 81.8 us -> 73.4 us
  local copies, waits for them, and re-layouts: 9.89 us -> 3.14 us
    pallas_call x1, Pallas kernels: 81.8 us -> 73.4 us  [local(): pl.pallas_call(functools.partial(kernel, cfg), name='whole', out_shape=(j...]
    unnamed x6 -> x2, local copies, waits for them, and re-layouts: 9.89 us -> 3.14 us
where the time goes in v2:
time: 77.8 us; the launch traced here: 77.2 us
  Pallas kernels  73.4 us (94%)
  local copies, waits for them, and re-layouts  3.14 us (4%)
    pallas_call x1, Pallas kernels, local(): pl.pallas_call(functools.partial(kernel, cfg), name='whole', out_shape=(j...  73.4 us
    unnamed x2, local copies, waits for them, and re-layouts  3.14 us

profile of v2, /device:TPU:2, one launch (start us, length us, event | category | flops | bytes accessed | tf_op | source)
XLA Modules:
  0.0 77.2 jit_solution(15742690787205312954)
XLA Ops:
  0.6 73.4 %whole.1 = (bf16[64,2048]{1,0:T(8,128)(2,1)}, bf16[128,256]{1,0:T(8,128)(2,1)}) custom-call(bf16[512,2048]{1,0:T(8,128)(2,1)} %refs_0_.1, f32[1,2048]{1,0:T(1,128)} %bitcast.9, bf16[2048,128]{1,0:T(8,128)(2,1)} %refs_2_.1, bf16[64,2048]{1,0:T(8,128)(2,1)} %bitcast.7, bf16[64,2048]{1,0:T(8,128)(2,1)} %bitcast.8, f32[1,2]{1,0:T(1,128)} %bitcast.13, ...), custom_call_target="tpu_custom_call" | custom-call | tf_op jit(solution)/shard_map/whole/pallas_call | solution.py:610
  74.1 1.7 %copy.25 = bf16[64,2048]{1,0:T(8,128)(2,1)} copy(bf16[64,2048]{1,0:T(8,128)(2,1)} %get-tuple-element.4) | data formatting | bytes 524288
  75.7 1.5 %copy.26 = bf16[128,256]{1,0:T(8,128)(2,1)} copy(bf16[128,256]{1,0:T(8,128)(2,1)} %get-tuple-element.5) | data formatting | bytes 131072

commit v3 on v2

--- a/solution.py
+++ b/solution.py
@@ -21,9 +21,8 @@
 
 
 CHUNK_Z = ((0, 1), (4, -2), (3, -3), (2,), (-1,))
-SHARED = (2, 2, 0, 0, 0)
-FAR_DIRECT = (0,)
-SEND_ORDER = ((0, 0), (0, 1), (1, 0), (2, 0), (3, 0), (4, 0))
+FAR_DIRECT = (2, 3, 4)
+SEND_ORDER = ((0, 0), (1, 0), (2, 0), (3, 0), (4, 0), (2, 1), (3, 1), (4, 1))
 
 
 def rope_tables(rows, n_ep):
@@ -43,24 +42,24 @@
         tok1_h, gain1_h, wq_h, wk_h, wv_h, sink_h, wo_h, tok2_h, gain2_h, routes_h, rw_h,
         wg_h, wu_h, wd_h, sg_h, su_h, sd_h, cosb_h, sinb_h, cosa_h, sina_h,
     ) = refs[:n_in]
-    mix_h, moe_h = refs[n_in : n_in + 2]
+    mix_o, moe_o = refs[n_in : n_in + 2]
     (
         tok1, gain1, wq, wk, wv, sink, wo, tok2, gain2, routes, rw,
         wg, wu, wd, sg, su, sd, cosb, sinb, cosa, sina,
     ) = refs[n_in + 2 : 2 * n_in + 2]
     (
         n2, comb, outgoing, xs, nrm, qs, kv, wkv, wof, att, attx, p_ref, pr, r2, r1, y_ref, ret, shr,
-        acc, mix_o, moe_o,
-        load_sem, halo_s, halo_r, dsp_s, dsp_r, ag_s, ag_r, rs_s, rs_r, wo_s, wo_r, at_s, at_r, rt_s, rt_r, st_sem,
+        acc,
+        load_sem, halo_s, halo_r, dsp_s, dsp_r, ag_s, ag_r, rs_s, rs_r, wo_s, wo_r, at_s, at_r, rt_s, rt_r,
     ) = refs[2 * n_in + 2 :]
     f = d_model // n_tp
     n_ep = nz * nx
     chunks = len(CHUNK_Z)
     slots_of = [nx * len(c) for c in CHUNK_Z]
-    groups_of = [a + b for a, b in zip(slots_of, SHARED)]
+    groups_of = slots_of + [t2 // (2 * CAP)]
     half_of = [g // 2 for g in groups_of]
-    piece = 2 * CAP
-    shared_at = [piece * sum(SHARED[:k]) for k in range(chunks)]
+    home = [k for k in range(chunks) if 0 in CHUNK_Z[k]][0]
+    home_q = CHUNK_Z[home].index(0)
 
     ep = lax.axis_index("ep")
     tp = lax.axis_index("tp")
@@ -134,7 +133,7 @@
         send(kv.at[pl.ds(t1, BAND)], kv.at[pl.ds(0, BAND)], halo_s, halo_r, (ep + 1) % n_ep, tp)
 
         for far_one, column in enumerate((tp, far)):
-            xs[0, column, x] = outgoing[far_one, ep]
+            xs[home, column, home_q * nx + x] = outgoing[far_one, ep]
         for k, far_one in SEND_ORDER:
             for q, dz in enumerate(CHUNK_Z[k]):
                 to_z = (z + nz - dz) % nz
@@ -170,7 +169,7 @@
         return pl.ds(0, slots_of[k] // 2), pl.ds(slots_of[k] // 2, slots_of[k] // 2)
 
     def dispatched(k, far_one):
-        first = 1 if k == 0 else 0
+        first = 1 if k == home else 0
         arrived(xs.at[k, 0, pl.ds(0, slots_of[k] - first)], dsp_r.at[k, far_one])
 
     def gather_start(k):
@@ -279,11 +278,9 @@
     def rs_end(k):
         total = ring_end(p_ref.at[k], r1.at[k], rs_r.at[k], half_of[k], groups_of[k])
         n_slots = slots_of[k]
-        y_ref[k, pl.ds(0, n_slots)] = total[:n_slots].astype(BF16)
-        if SHARED[k]:
-            shr[pl.ds(shared_at[k], SHARED[k] * piece)] = total[n_slots:].reshape(SHARED[k] * piece, f)
-        if k == 0:
-            ret[z, x] = y_ref[0, x]
+        y_ref[k, pl.ds(0, n_slots)] = total.astype(BF16)
+        if k == home:
+            ret[z, x] = y_ref[k, home_q * nx + x]
         for q, dz in enumerate(CHUNK_Z[k]):
             src_z = (z + nz + dz) % nz
             for i in range(nx):
@@ -296,7 +293,7 @@
                 ).start()
 
     def combine(k):
-        first = 1 if k == 0 else 0
+        first = 1 if k == home else 0
         arrived(y_ref.at[k, pl.ds(0, slots_of[k] - first)], rt_r.at[k])
         total = jnp.zeros((t2, f), F32)
         for dz in CHUNK_Z[k]:
@@ -318,10 +315,15 @@
         hidden = (gate / (1.0 + jnp.exp(-gate)) * up_pre).astype(BF16)
         for j in range(n_tp):
             res = jnp.dot(hidden, sd[:, j * f : (j + 1) * f], preferred_element_type=F32).astype(BF16)
-            for k in range(chunks):
-                if SHARED[k]:
-                    rows_k = res[shared_at[k] : shared_at[k] + SHARED[k] * piece]
-                    p_ref[k, j // 2, j % 2, pl.ds(slots_of[k], SHARED[k])] = rows_k.reshape(SHARED[k], 2, CAP, f)
+            p_ref[chunks, j // 2, j % 2, pl.ds(0, groups_of[chunks])] = res.reshape(groups_of[chunks], 2, CAP, f)
+
+    def shared_send():
+        k = chunks
+        pair_send(p_ref.at[k], pr.at[k], rs_s.at[k], rs_r.at[k], groups_of[k])
+
+    def shared_end():
+        k = chunks
+        shr[...] = ring_end(p_ref.at[k], r1.at[k], rs_r.at[k], half_of[k], groups_of[k]).reshape(t2, f)
 
     blk = BAND
     n_blk = t1 // blk
@@ -393,10 +395,10 @@
 
     def project_first():
         wait_loads(0, 1, 2, 3, 4, 5, 17, 18, 19, 20)
-        lax.fori_loop(0, n_blk - 1, project, 0)
+        project(0, 0)
 
     def project_last():
-        project(n_blk - 1, 0)
+        lax.fori_loop(1, n_blk, project, 0)
 
     def attend_rest(b, carry):
         attend(b)
@@ -475,69 +477,74 @@
             return carry
 
         lax.fori_loop(0, d_model // n_cols, columns, 0)
-        store = pltpu.make_async_copy(mix_o, mix_h, st_sem.at[0])
-        store.start()
-        return store
 
     stage("project", project_first)
     stage("dispatch", dispatch_all)
     stage("w_y_start", weight_y_start)
     stage("project_last", project_last)
+    stage("ag_start0", gather_start, 0)
+    stage("shared", shared)
+    stage("shared_send", shared_send)
+    stage("w_y_fwd", weight_y_forward)
     stage("attend", attend_later)
-    stage("ag_start0", gather_start, 0)
-    stage("w_y_fwd", weight_y_forward)
-    stage("attend0", attend_first)
     stage("ag_start1", gather_start, 1)
     stage("ag_fwd0", gather_forward, 0)
-    stage("shared", shared)
+    stage("shared_first", rs_first, chunks)
+    stage("ag_start2", gather_start, 2)
+    stage("attend0", attend_first)
+    stage("ag_far0", gather_far, 0)
+    stage("shared_second", rs_second, chunks)
     stage("w_x_start", weight_x_start)
-    stage("ag_far0", gather_far, 0)
-    stage("ag_start2", gather_start, 2)
     stage("ag_fwd1", gather_forward, 1)
     stage("load_w", wait_loads, 11, 12, 13)
     stage("ag_end0", gather_end, 0)
     stage("experts0", experts, 0)
-    stage("weights", combine_weights)
     stage("ag_start3", gather_start, 3)
     stage("ag_start4", gather_start, 4)
+    stage("ag_far1", gather_far, 1)
+    stage("ag_fwd2", gather_forward, 2)
     stage("rs_first0", rs_first, 0)
-    stage("ag_far1", gather_far, 1)
-    store_mix = None
-    for k in range(1, chunks):
-        if k + 1 < chunks:
-            stage(f"ag_fwd{k + 1}", gather_forward, k + 1)
-        if k >= 2:
-            stage(f"rs_first{k - 1}", rs_first, k - 1)
-        stage(f"ag_end{k}", gather_end, k)
-        stage(f"experts{k}", experts, k)
-        if k + 1 < chunks:
-            stage(f"ag_far{k + 1}", gather_far, k + 1)
-        if k == 1:
-            stage("w_x_fwd", weight_x_forward)
-        if k == 2:
-            stage("w_x_far", weight_x_far)
-        stage(f"rs_second{k - 1}", rs_second, k - 1)
-        if k == 3:
-            store_mix = stage("mix_end", mixer_end)
-        if k >= 2:
-            stage(f"rs_end{k - 2}", rs_end, k - 2)
-    last = chunks - 1
-    stage(f"rs_first{last}", rs_first, last)
-    stage(f"rs_end{last - 1}", rs_end, last - 1)
-    stage(f"rs_second{last}", rs_second, last)
-    stage("combine0", combine, 0)
-    stage(f"rs_end{last}", rs_end, last)
-    for k in range(1, chunks):
+    stage("ag_end1", gather_end, 1)
+    stage("experts1", experts, 1)
+    stage("ag_fwd3", gather_forward, 3)
+    stage("ag_fwd4", gather_forward, 4)
+    stage("ag_far2", gather_far, 2)
+    stage("weights", combine_weights)
+    stage("rs_first1", rs_first, 1)
+    stage("rs_second0", rs_second, 0)
+    stage("ag_end2", gather_end, 2)
+    stage("experts2", experts, 2)
+    stage("w_x_fwd", weight_x_forward)
+    stage("ag_far3", gather_far, 3)
+    stage("ag_far4", gather_far, 4)
+    stage("ag_end3", gather_end, 3)
+    stage("experts3", experts, 3)
+    stage("rs_first2", rs_first, 2)
+    stage("rs_second1", rs_second, 1)
+    stage("rs_end0", rs_end, 0)
+    stage("ag_end4", gather_end, 4)
+    stage("experts4", experts, 4)
+    stage("shared_end", shared_end)
+    stage("rs_first3", rs_first, 3)
+    stage("rs_first4", rs_first, 4)
+    stage("rs_second2", rs_second, 2)
+    stage("rs_end1", rs_end, 1)
+    stage("rs_second3", rs_second, 3)
+    stage("rs_second4", rs_second, 4)
+    stage("rs_end2", rs_end, 2)
+    stage("w_x_far", weight_x_far)
+    stage("rs_end3", rs_end, 3)
+    stage("rs_end4", rs_end, 4)
+    stage("mix_end", mixer_end)
+    for k in range(chunks):
         stage(f"combine{k}", combine, k)
 
     def finish():
         moe_o[...] = (acc[...] + shr[...]).astype(BF16)
-        store_moe = pltpu.make_async_copy(moe_o, moe_h, st_sem.at[1])
-        store_moe.start()
         for src, sem in sends:
             pltpu.make_async_copy(src, src, sem).wait()
         whole = outgoing.at[0, pl.ds(0, n_ep - 1)]
-        sent_far = sum(slots_of[k] for k in FAR_DIRECT) - (1 if 0 in FAR_DIRECT else 0)
+        sent_far = sum(slots_of[k] for k in FAR_DIRECT) - (1 if home in FAR_DIRECT else 0)
         pltpu.make_async_copy(whole, whole, dsp_s).wait()
         if sent_far:
             far_part = outgoing.at[1, pl.ds(0, sent_far)]
@@ -545,8 +552,6 @@
         pltpu.make_async_copy(whole, whole, rt_s).wait()
         rows_out = attx.at[pl.ds(0, n_tp - 1)]
         pltpu.make_async_copy(rows_out, rows_out, at_s).wait()
-        store_mix.wait()
-        store_moe.wait()
 
     stage("finish", finish)
 
@@ -564,7 +569,7 @@
         f = d_model // n_tp
         chunks = len(CHUNK_Z)
         slot_groups = nx * max(len(c) for c in CHUNK_Z)
-        groups = max(nx * len(c) + b for c, b in zip(CHUNK_Z, SHARED))
+        groups = max(slot_groups, t2 // (2 * CAP))
         half = (groups + 1) // 2
         rows_tp = t1 // n_tp
         tables = tuple(jnp.asarray(t) for t in rope_tables(t1, n_ep))
@@ -586,25 +591,22 @@
             vm((nx, 2, NY, 128 // nx, d_model), BF16),
             vm((t1, 128), BF16),
             vm((n_tp, rows_tp, 128), BF16),
-            vm((chunks, NY, 2, groups, 2, CAP, f), BF16),
-            vm((chunks, NY, groups, 2, CAP, f), BF16),
-            vm((chunks, 2, half, 2, CAP, f), BF16),
-            vm((chunks, 2, groups, 2, CAP, f), BF16),
+            vm((chunks + 1, NY, 2, groups, 2, CAP, f), BF16),
+            vm((chunks + 1, NY, groups, 2, CAP, f), BF16),
+            vm((chunks + 1, 2, half, 2, CAP, f), BF16),
+            vm((chunks + 1, 2, groups, 2, CAP, f), BF16),
             vm((chunks, slot_groups, 2, CAP, f), BF16),
             vm((nz, nx, 2, CAP, f), BF16),
             vm((t2, f), F32),
             vm((t2, f), F32),
-            vm((rows_tp, d_model), BF16),
-            vm((t2, f), BF16),
             dma((len(args),)),
             dma, dma,
             dma, dma((chunks, 2)),
             dma((chunks, 9)), dma((chunks, 9)),
-            dma((chunks, 10)), dma((chunks, 10)),
+            dma((chunks + 1, 10)), dma((chunks + 1, 10)),
             dma((13,)), dma((13,)),
             dma, dma,
             dma, dma((chunks,)),
-            dma((2,)),
         ]
         cfg = (nz, nx, n_tp, d_model, t1, t2, topk, eff, sff)
         return pl.pallas_call(
@@ -614,14 +616,13 @@
                 jax.ShapeDtypeStruct((rows_tp, d_model), BF16),
                 jax.ShapeDtypeStruct((t2, f), BF16),
             ),
-            in_specs=[pl.BlockSpec(memory_space=pl.ANY)] * len(args),
-            out_specs=(pl.BlockSpec(memory_space=pl.ANY),) * 2,
+            in_specs=[pl.BlockSpec(memory_space=pltpu.HBM)] * len(args),
+            out_specs=(pl.BlockSpec(memory_space=pltpu.VMEM),) * 2,
             scratch_shapes=scratch,
             compiler_params=pltpu.CompilerParams(
-                collective_id=0, has_side_effects=True, vmem_limit_bytes=60 * 1024 * 1024
+                collective_id=0, has_side_effects=True, vmem_limit_bytes=44 * 1024 * 1024
             ),
-        )(*args)
-
+        )(*[pltpu.with_memory_space_constraint(a, pltpu.HBM) for a in args])
     in_specs = (
         P("ep", None), P(), P(None, "tp"), P(None, "tp"), P(None, "tp"), P("tp"), P("tp", None),
         P("ep", None), P(), P("ep", None), P("ep", None),

time: 77.8 us -> 72.6 us (0.933)
  Pallas kernels: 73.4 us -> 69.7 us
  local copies, waits for them, and re-layouts: 3.14 us -> 1.33 us
    pallas_call x1, Pallas kernels: 73.4 us -> 69.7 us  [local(): pl.pallas_call(functools.partial(kernel, cfg), name='whole', out_shape=(j...]
    unnamed x2, local copies, waits for them, and re-layouts: 3.14 us -> 1.33 us
where the time goes in v3:
time: 72.6 us; the launch traced here: 71.7 us
  Pallas kernels  69.7 us (96%)
  local copies, waits for them, and re-layouts  1.33 us (2%)
    pallas_call x1, Pallas kernels, local(): pl.pallas_call(functools.partial(kernel, cfg), name='whole', out_shape=(j...  69.7 us

profile of v3, /device:TPU:2, one launch (start us, length us, event | category | flops | bytes accessed | tf_op | source)
XLA Modules:
  0.0 71.7 jit_solution(13076702165105033393)
XLA Ops:
  0.6 69.7 %whole.1 = (bf16[64,2048]{1,0:T(8,128)(2,1)S(1)}, bf16[128,256]{1,0:T(8,128)(2,1)S(1)}) custom-call(bf16[512,2048]{1,0:T(8,128)(2,1)} %refs_0_.1, f32[1,2048]{1,0:T(1,128)} %bitcast.9, bf16[2048,128]{1,0:T(8,128)(2,1)} %refs_2_.1, bf16[64,2048]{1,0:T(8,128)(2,1)} %bitcast.7, bf16[64,2048]{1,0:T(8,128)(2,1)} %bitcast.8, f32[1,2]{1,0:T(1,128)} %bitcast.13, ...), custom_call_target="tpu_custom_call" | custom-call | tf_op jit(solution)/shard_map/whole/pallas_call | solution.py:612
  70.3 0.7 copy.25
  71.0 0.6 copy.26

commit v4 on v3

--- a/solution.py
+++ b/solution.py
@@ -21,8 +21,8 @@
 
 
 CHUNK_Z = ((0, 1), (4, -2), (3, -3), (2,), (-1,))
-FAR_DIRECT = (2, 3, 4)
-SEND_ORDER = ((0, 0), (1, 0), (2, 0), (3, 0), (4, 0), (2, 1), (3, 1), (4, 1))
+FAR_DIRECT = (0, 2, 3, 4)
+SEND_ORDER = ((0, 0), (0, 1), (1, 0), (2, 0), (3, 0), (4, 0), (2, 1), (3, 1), (4, 1))
 
 
 def rope_tables(rows, n_ep):
@@ -490,15 +490,15 @@
     stage("ag_start1", gather_start, 1)
     stage("ag_fwd0", gather_forward, 0)
     stage("shared_first", rs_first, chunks)
+    stage("ag_far0", gather_far, 0)
     stage("ag_start2", gather_start, 2)
-    stage("attend0", attend_first)
-    stage("ag_far0", gather_far, 0)
     stage("shared_second", rs_second, chunks)
     stage("w_x_start", weight_x_start)
     stage("ag_fwd1", gather_forward, 1)
     stage("load_w", wait_loads, 11, 12, 13)
     stage("ag_end0", gather_end, 0)
     stage("experts0", experts, 0)
+    stage("attend0", attend_first)
     stage("ag_start3", gather_start, 3)
     stage("ag_start4", gather_start, 4)
     stage("ag_far1", gather_far, 1)
@@ -509,35 +509,38 @@
     stage("ag_fwd3", gather_forward, 3)
     stage("ag_fwd4", gather_forward, 4)
     stage("ag_far2", gather_far, 2)
+    stage("rs_second0", rs_second, 0)
     stage("weights", combine_weights)
     stage("rs_first1", rs_first, 1)
-    stage("rs_second0", rs_second, 0)
     stage("ag_end2", gather_end, 2)
     stage("experts2", experts, 2)
+    stage("rs_end0", rs_end, 0)
     stage("w_x_fwd", weight_x_forward)
     stage("ag_far3", gather_far, 3)
     stage("ag_far4", gather_far, 4)
+    stage("rs_second1", rs_second, 1)
+    stage("rs_first2", rs_first, 2)
     stage("ag_end3", gather_end, 3)
     stage("experts3", experts, 3)
-    stage("rs_first2", rs_first, 2)
-    stage("rs_second1", rs_second, 1)
-    stage("rs_end0", rs_end, 0)
+    stage("rs_end1", rs_end, 1)
+    stage("rs_second2", rs_second, 2)
+    stage("rs_first3", rs_first, 3)
     stage("ag_end4", gather_end, 4)
     stage("experts4", experts, 4)
+    stage("rs_end2", rs_end, 2)
+    stage("rs_second3", rs_second, 3)
+    stage("rs_first4", rs_first, 4)
     stage("shared_end", shared_end)
-    stage("rs_first3", rs_first, 3)
-    stage("rs_first4", rs_first, 4)
-    stage("rs_second2", rs_second, 2)
-    stage("rs_end1", rs_end, 1)
-    stage("rs_second3", rs_second, 3)
-    stage("rs_second4", rs_second, 4)
-    stage("rs_end2", rs_end, 2)
     stage("w_x_far", weight_x_far)
     stage("rs_end3", rs_end, 3)
+    stage("rs_second4", rs_second, 4)
     stage("rs_end4", rs_end, 4)
     stage("mix_end", mixer_end)
-    for k in range(chunks):
-        stage(f"combine{k}", combine, k)
+    stage("combine0", combine, 0)
+    stage("combine1", combine, 1)
+    stage("combine2", combine, 2)
+    stage("combine3", combine, 3)
+    stage("combine4", combine, 4)
 
     def finish():
         moe_o[...] = (acc[...] + shr[...]).astype(BF16)

time: 72.6 us -> 68.7 us (0.946); the launches traced: 71.7 us -> 68.6 us
  Pallas kernels: 69.7 us -> 66.6 us
    pallas_call x1, Pallas kernels: 69.7 us -> 66.6 us  [local(): pl.pallas_call(functools.partial(kernel, cfg), name='whole', out_shape=(j...]
where the time goes in v4:
time: 68.7 us; the launch traced here: 68.6 us
  Pallas kernels  66.6 us (97%)
  local copies, waits for them, and re-layouts  1.33 us (2%)
    pallas_call x1, Pallas kernels, local(): pl.pallas_call(functools.partial(kernel, cfg), name='whole', out_shape=(j...  66.6 us

profile of v4, /device:TPU:2, one launch (start us, length us, event | category | flops | bytes accessed | tf_op | source)
XLA Modules:
  0.0 68.6 jit_solution(10666291137491939741)
XLA Ops:
  0.6 66.6 %whole.1 = (bf16[64,2048]{1,0:T(8,128)(2,1)S(1)}, bf16[128,256]{1,0:T(8,128)(2,1)S(1)}) custom-call(bf16[512,2048]{1,0:T(8,128)(2,1)} %refs_0_.1, f32[1,2048]{1,0:T(1,128)} %bitcast.9, bf16[2048,128]{1,0:T(8,128)(2,1)} %refs_2_.1, bf16[64,2048]{1,0:T(8,128)(2,1)} %bitcast.7, bf16[64,2048]{1,0:T(8,128)(2,1)} %bitcast.8, f32[1,2]{1,0:T(1,128)} %bitcast.13, ...), custom_call_target="tpu_custom_call" | custom-call | tf_op jit(solution)/shard_map/whole/pallas_call | solution.py:615
  67.3 0.7 %copy.25 = bf16[64,2048]{1,0:T(8,128)(2,1)} copy(bf16[64,2048]{1,0:T(8,128)(2,1)S(1)} %get-tuple-element.4) | data formatting | bytes 524288
  68.0 0.6 copy.26

commit v5 on v4

--- a/solution.py
+++ b/solution.py
@@ -493,47 +493,47 @@
     stage("ag_far0", gather_far, 0)
     stage("ag_start2", gather_start, 2)
     stage("shared_second", rs_second, chunks)
-    stage("w_x_start", weight_x_start)
     stage("ag_fwd1", gather_forward, 1)
     stage("load_w", wait_loads, 11, 12, 13)
     stage("ag_end0", gather_end, 0)
     stage("experts0", experts, 0)
+    stage("w_x_start", weight_x_start)
     stage("attend0", attend_first)
+    stage("weights", combine_weights)
     stage("ag_start3", gather_start, 3)
     stage("ag_start4", gather_start, 4)
+    stage("rs_first0", rs_first, 0)
     stage("ag_far1", gather_far, 1)
     stage("ag_fwd2", gather_forward, 2)
-    stage("rs_first0", rs_first, 0)
     stage("ag_end1", gather_end, 1)
     stage("experts1", experts, 1)
     stage("ag_fwd3", gather_forward, 3)
     stage("ag_fwd4", gather_forward, 4)
     stage("ag_far2", gather_far, 2)
     stage("rs_second0", rs_second, 0)
-    stage("weights", combine_weights)
     stage("rs_first1", rs_first, 1)
     stage("ag_end2", gather_end, 2)
     stage("experts2", experts, 2)
     stage("rs_end0", rs_end, 0)
-    stage("w_x_fwd", weight_x_forward)
     stage("ag_far3", gather_far, 3)
     stage("ag_far4", gather_far, 4)
     stage("rs_second1", rs_second, 1)
     stage("rs_first2", rs_first, 2)
     stage("ag_end3", gather_end, 3)
     stage("experts3", experts, 3)
+    stage("ag_end4", gather_end, 4)
+    stage("experts4", experts, 4)
+    stage("w_x_fwd", weight_x_forward)
     stage("rs_end1", rs_end, 1)
     stage("rs_second2", rs_second, 2)
     stage("rs_first3", rs_first, 3)
-    stage("ag_end4", gather_end, 4)
-    stage("experts4", experts, 4)
+    stage("rs_first4", rs_first, 4)
     stage("rs_end2", rs_end, 2)
     stage("rs_second3", rs_second, 3)
-    stage("rs_first4", rs_first, 4)
+    stage("rs_second4", rs_second, 4)
     stage("shared_end", shared_end)
+    stage("rs_end3", rs_end, 3)
     stage("w_x_far", weight_x_far)
-    stage("rs_end3", rs_end, 3)
-    stage("rs_second4", rs_second, 4)
     stage("rs_end4", rs_end, 4)
     stage("mix_end", mixer_end)
     stage("combine0", combine, 0)

time: 68.7 us -> 66.7 us (0.971)
  Pallas kernels: 66.6 us -> 64.3 us
    pallas_call x1, Pallas kernels: 66.6 us -> 64.3 us  [local(): pl.pallas_call(functools.partial(kernel, cfg), name='whole', out_shape=(j...]
where the time goes in v5:
time: 66.7 us; the launch traced here: 66.3 us
  Pallas kernels  64.3 us (96%)
  local copies, waits for them, and re-layouts  1.33 us (2%)
    pallas_call x1, Pallas kernels, local(): pl.pallas_call(functools.partial(kernel, cfg), name='whole', out_shape=(j...  64.3 us
    unnamed x2, local copies, waits for them, and re-layouts  1.33 us

profile of v5, /device:TPU:2, one launch (start us, length us, event | category | flops | bytes accessed | tf_op | source)
XLA Modules:
  0.0 66.3 jit_solution(9986394306154687829)
XLA Ops:
  0.6 64.3 %whole.1 = (bf16[64,2048]{1,0:T(8,128)(2,1)S(1)}, bf16[128,256]{1,0:T(8,128)(2,1)S(1)}) custom-call(bf16[512,2048]{1,0:T(8,128)(2,1)} %refs_0_.1, f32[1,2048]{1,0:T(1,128)} %bitcast.9, bf16[2048,128]{1,0:T(8,128)(2,1)} %refs_2_.1, bf16[64,2048]{1,0:T(8,128)(2,1)} %bitcast.7, bf16[64,2048]{1,0:T(8,128)(2,1)} %bitcast.8, f32[1,2]{1,0:T(1,128)} %bitcast.13, ...), custom_call_target="tpu_custom_call" | custom-call | tf_op jit(solution)/shard_map/whole/pallas_call | solution.py:615
  65.0 0.7 %copy.25 = bf16[64,2048]{1,0:T(8,128)(2,1)} copy(bf16[64,2048]{1,0:T(8,128)(2,1)S(1)} %get-tuple-element.4) | data formatting | bytes 524288
  65.7 0.6 copy.26
